TPU v7x, 128 devices: a whole 4x4x4 slice. The times are simulated.
128 devices in a mesh: fs: 16 (over z, x), tp: 8 (over y, core).
Axes of the slice: x: 4, y: 4, z: 4, core: 2. Of those that a mesh axis runs over, the one named last changes fastest.
Arguments:
- later_input: bfloat16 [12288, 2048], P('fs', 'tp'), may hold values from -6 to 6
- earlier_input: bfloat16 [12288, 2048], P('fs', 'tp'), may hold values from -6 to 6
- cotangent: bfloat16 [12288, 2048], P('fs', 'tp'), may hold values from -6 to 6
- up_weight: bfloat16 [2048, 8192], P('fs', 'tp'), may hold values from -0.125 to 0.125
- down_weight: bfloat16 [8192, 2048], P('tp', 'fs'), may hold values from -0.0625 to 0.0625
- up_running: float32 [2048, 8192], P('fs', 'tp'), may hold values from -6 to 6
- down_running: float32 [2048, 8192], P('fs', 'tp'), may hold values from -6 to 6
Outputs:
- later_output: bfloat16 [12288, 2048], P('fs', 'tp')
- later_preact: bfloat16 [12288, 8192], P('fs', 'tp')
- earlier_grad: bfloat16 [12288, 2048], P('fs', 'tp')
- up_running_out: float32 [2048, 8192], P('fs', 'tp')
- down_running_out: float32 [2048, 8192], P('fs', 'tp')
All inputs are finite; a program needn't handle non-finite values.
Results may differ from a plain program's by a relative error of at most 0.014.
Values may be sent and summed in bfloat16 or wider, within the bound.
A program may use at most 128 MiB of HBM per device.

v0:
```python
import jax
import jax.numpy as jnp
from jax import lax
from jax.sharding import PartitionSpec as P

contract_last = (((1,), (1,)), ((), ()))
contract_first = (((0,), (0,)), ((), ()))


def in_one_piece(arrays, axis, dim, along):
    ends, at = ([], 0)
    for a in arrays[:-1]:
        at += a.shape[along]
        ends.append(at)
    both = jnp.concatenate(arrays, axis=along)
    return tuple(jnp.split(lax.all_gather(both, axis, axis=dim, tiled=True), ends, axis=along))


def gather_turned(arrays, axis, dims):
    turned = [jnp.moveaxis(a, dim, 0) for a, dim in zip(arrays, dims)]
    widths = [t[0].size for t in turned]
    both = jnp.concatenate([t.reshape(-1, w) for t, w in zip(turned, widths)], axis=1)
    filled = lax.all_gather(both, axis, axis=0, tiled=True)
    tiles = jnp.split(filled, [sum(widths[:k]) for k in range(1, len(widths))], axis=1)
    return tuple(
        (
            jnp.moveaxis(b.reshape(-1, *t.shape[1:]), 0, dim)
            for b, t, dim in zip(tiles, turned, dims)
        )
    )


def side_by_side(arrays, axis, dim, along):
    both = jnp.concatenate(arrays, axis=along)
    filled, at, outs = (lax.psum_scatter(both, axis, scatter_dimension=dim, tiled=True), 0, [])
    for a in arrays:
        outs.append(lax.slice_in_dim(filled, at, at + a.shape[along], axis=along))
        at += a.shape[along]
    return tuple(outs)


def on_device(
    later_input, earlier_input, cotangent, up_weight, down_weight, up_running, down_running
):
    rows = later_input.shape[0]
    factor = float(rows * lax.axis_size("fs")) ** (-0.5)
    later_full, earlier_full, cot_full = in_one_piece(
        (later_input, earlier_input, cotangent), "tp", 1, 0
    )
    columns = up_weight.shape[1]
    up_whole, down_whole = gather_turned((up_weight, down_weight), "fs", (0, 1))
    later_up = jnp.dot(later_full, up_whole, preferred_element_type=jnp.float32)
    earlier_up = jnp.dot(earlier_full, up_whole, preferred_element_type=jnp.float32)
    later_hidden = jnp.square(jax.nn.relu(later_up)).astype(jnp.bfloat16)
    out_part = jnp.dot(later_hidden, down_whole, preferred_element_type=jnp.float32)
    hidden_grad = lax.dot_general(
        cot_full, down_whole, contract_last, preferred_element_type=jnp.float32
    )
    up_grad = (2.0 * jax.nn.relu(earlier_up) * hidden_grad).astype(jnp.bfloat16)
    back_part = lax.dot_general(
        up_grad, up_whole, contract_last, preferred_element_type=jnp.float32
    )
    later_preact = later_up.astype(jnp.bfloat16)
    earlier_hidden = jnp.square(jax.nn.relu(earlier_up)).astype(jnp.bfloat16)
    out_sum, back_sum = tuple(
        (
            part.astype(jnp.float32)
            for part in side_by_side(
                (out_part.astype(jnp.bfloat16), back_part.astype(jnp.bfloat16)), "tp", 1, 0
            )
        )
    )
    summed = lax.psum_scatter(
        jnp.concatenate(
            (
                lax.dot_general(
                    earlier_full, up_grad, contract_first, preferred_element_type=jnp.float32
                ),
                lax.dot_general(
                    cot_full, earlier_hidden, contract_first, preferred_element_type=jnp.float32
                ),
            ),
            axis=1,
        ).astype(jnp.bfloat16),
        "fs",
        scatter_dimension=0,
        tiled=True,
    ).astype(jnp.float32)
    grad_up_sum = summed[:, :columns]
    grad_down_sum = summed[:, columns:]
    return (
        out_sum.astype(jnp.bfloat16),
        later_preact,
        back_sum.astype(jnp.bfloat16),
        up_running + grad_up_sum * factor,
        down_running + grad_down_sum * factor,
    )


def solution(mesh):
    in_specs = (
        P("fs", "tp"),
        P("fs", "tp"),
        P("fs", "tp"),
        P("fs", "tp"),
        P("tp", "fs"),
        P("fs", "tp"),
        P("fs", "tp"),
    )
    out_specs = (P("fs", "tp"), P("fs", "tp"), P("fs", "tp"), P("fs", "tp"), P("fs", "tp"))
    return jax.shard_map(
        on_device, mesh=mesh, in_specs=in_specs, out_specs=out_specs, check_vma=False
    )
```

profile of v0, /device:TPU:0, one launch (start us, length us, event | category | flops | bytes accessed | tf_op | source)
XLA Modules:
  0.0 322.6 jit_solution(7393562719880853422)
XLA Ops:
  7.2 1.1 copy.17
  8.3 1.8 pad_maximum_fusion.3
  10.2 2.3 pad_maximum_fusion.2
  12.6 77.9 %all-gather.5.cloned.1.call-done = bf16[2048,2048]{0,1:T(8,128)(2,1)} async-done(((bf16[128,2048]{0,1:T(8,128)(2,1)}), bf16[2048,2048]{0,1:T(8,128)(2,1)}) %all-gather.5.cloned.1.call-update) | async-done | bytes 8388624 | tf_op jit(solution)/shard_map/all_gather | solution.py:23
  90.5 59.5 %all-gather.3.cloned.1.call-done = bf16[2304,2048]{1,0:T(8,128)(2,1)} async-done(((bf16[2304,256]{1,0:T(8,128)(2,1)}), bf16[2304,2048]{1,0:T(8,128)(2,1)}) %all-gather.3.cloned.1.call-update) | async-done | bytes 9437200 | tf_op jit(solution)/shard_map/all_gather | solution.py:16
  150.0 6.3 %fusion.8 = f32[768,1024]{1,0:T(8,128)S(1)} fusion(bf16[2048,2048]{0,1:T(8,128)(2,1)} %all-gather.5.cloned.1.call-done, bf16[2304,2048]{1,0:T(8,128)(2,1)} %all-gather.3.cloned.1.call-done), kind=kOutput, calls=%fused_computation.11 | convolution fusion | flops 3221225472 | bytes 10485760 | tf_op jit(solution)/shard_map/dot_general | solution.py:53
  156.4 1.9 copy-done.3
  158.3 4.7 %fusion.28 = (bf16[768,1024]{1,0:T(8,128)(2,1)}, f32[768,1024]{1,0:T(8,128)S(1)}) fusion(bf16[2048,2048]{0,1:T(8,128)(2,1)S(1)} %copy-done.3, bf16[2304,2048]{1,0:T(8,128)(2,1)S(1)} %copy-done.2), kind=kOutput, calls=%fused_computation.34 | convolution fusion | flops 3222011904 | bytes 12058624 | tf_op jit(solution)/shard_map/dot_general | solution.py:52
  163.0 3.6 %multiply_convert_fusion.1 = bf16[768,1024]{1,0:T(8,128)(2,1)S(1)} fusion(f32[768,1024]{1,0:T(8,128)S(1)} %fusion.8, bf16[2048,2048]{0,1:T(8,128)(2,1)S(1)} %copy-done.3, bf16[2304,2048]{1,0:T(8,128)(2,1)S(1)} %copy-done.2), kind=kOutput, calls=%fused_computation.17 | convolution fusion | flops 3224371200 | bytes 12058624 | tf_op jit(solution)/shard_map/dot_general | solution.py:56
  166.6 3.7 %convolution_convert_fusion.2 = bf16[768,2048]{1,0:T(8,128)(2,1)S(1)} fusion(bf16[768,1024]{1,0:T(8,128)(2,1)S(1)} %multiply_convert_fusion.1, bf16[2048,2048]{0,1:T(8,128)(2,1)S(1)} %copy-done.3), kind=kOutput, calls=%fused_computation.9 | convolution fusion | flops 3222798336 | bytes 8912896 | tf_op jit(solution)/shard_map/dot_general | solution.py:60
  170.2 5.9 %fusion.4 = bf16[768,2048]{1,0:T(8,128)(2,1)S(1)} fusion(bf16[2048,2048]{0,1:T(8,128)(2,1)} %all-gather.5.cloned.1.call-done, f32[768,1024]{1,0:T(8,128)S(1)} %get-tuple-element.20), kind=kOutput, calls=%fused_computation.8 | convolution fusion | flops 3225157632 | bytes 10485760 | tf_op jit(solution)/shard_map/dot_general | solution.py:55
  176.1 3.8 %pad_maximum_fusion.1 = bf16[1536,2048]{1,0:T(8,128)(2,1)} fusion(bf16[768,2048]{1,0:T(8,128)(2,1)S(1)} %convolution_convert_fusion.2, bf16[768,2048]{1,0:T(8,128)(2,1)S(1)} %fusion.4), kind=kLoop, calls=%fused_computation.1 | loop fusion | flops 12582912 | bytes 12582912 | tf_op jit(solution)/shard_map/concatenate | solution.py:34
  179.9 0.2 reduce-scatter.7.cloned.1.call-start
  180.2 8.0 %convolution_convert_fusion.1 = bf16[2048,1024]{0,1:T(8,128)(2,1)} fusion(bf16[768,1024]{1,0:T(8,128)(2,1)} %copy-done.6, bf16[2304,2048]{1,0:T(8,128)(2,1)} %all-gather.3.cloned.1.call-done), kind=kOutput, calls=%fused_computation.3 | convolution fusion | flops 3223322624 | bytes 8912896 | tf_op jit(solution)/shard_map/dot_general | solution.py:76
  188.2 7.3 %convolution_convert_fusion = bf16[2048,1024]{0,1:T(8,128)(2,1)} fusion(bf16[2304,2048]{1,0:T(8,128)(2,1)} %all-gather.3.cloned.1.call-done, f32[768,1024]{1,0:T(8,128)S(1)} %copy-done.5), kind=kOutput, calls=%fused_computation.2 | convolution fusion | flops 3225681920 | bytes 10485760 | tf_op jit(solution)/shard_map/dot_general | solution.py:79
  195.4 8.5 %pad_maximum_fusion = bf16[2048,2048]{0,1:T(8,128)(2,1)} fusion(bf16[2048,1024]{0,1:T(8,128)(2,1)} %convolution_convert_fusion, bf16[2048,1024]{0,1:T(8,128)(2,1)} %convolution_convert_fusion.1), kind=kLoop, calls=%fused_computation | loop fusion | flops 16777216 | bytes 16777216 | tf_op jit(solution)/shard_map/concatenate | solution.py:74
  204.0 12.3 %copy.22 = bf16[2048,2048]{1,0:T(8,128)(2,1)} copy(bf16[2048,2048]{0,1:T(8,128)(2,1)} %pad_maximum_fusion) | data formatting | bytes 16777216
  216.3 1.0 copy-done
  217.7 5.9 %reduce-scatter.5.cloned.1.call-done = bf16[1536,256]{1,0:T(8,128)(2,1)} async-done(((bf16[1536,2048]{1,0:T(8,128)(2,1)}), bf16[1536,256]{1,0:T(8,128)(2,1)}) %reduce-scatter.5.cloned.1.call-update) | async-done | bytes 786448 | tf_op jit(solution)/shard_map/reduce_scatter | solution.py:35
  223.6 2.0 fusion.27
  225.6 87.0 %reduce-scatter.7.cloned.1.call-done = bf16[128,2048]{1,0:T(8,128)(2,1)} async-done(((bf16[2048,2048]{1,0:T(8,128)(2,1)}), bf16[128,2048]{1,0:T(8,128)(2,1)}) %reduce-scatter.7.cloned.1.call-update) | async-done | bytes 524304
  312.6 1.3 copy.23
  314.1 1.0 copy.20
  315.1 1.0 copy.21
  (23 shorter events, 0.8 us)
Async XLA Ops:
  7.2 83.4 %all-gather.5.cloned.1.call-start = ((), (), s32[]{:S(2)}) async-start(), calls=%async_computation.3 | async-start | bytes 8912896 | tf_op jit(solution)/shard_map/all_gather | solution.py:23
  10.1 139.9 %all-gather.3.cloned.1.call-start = ((), (), s32[]{:S(2)}) async-start(), calls=%async_computation.2 | async-start | bytes 10616832 | tf_op jit(solution)/shard_map/all_gather | solution.py:16
  12.5 211.0 %reduce-scatter.5.cloned.1.call-start = ((), (), s32[]{:S(2)}) async-start(), calls=%async_computation.4 | async-start | bytes 7077888 | tf_op jit(solution)/shard_map/reduce_scatter | solution.py:35
  150.0 6.4 %copy-start.2 = (bf16[2304,2048]{1,0:T(8,128)(2,1)S(1)}, bf16[2304,2048]{1,0:T(8,128)(2,1)}, u32[]{:S(2)}) copy-start(bf16[2304,2048]{1,0:T(8,128)(2,1)} %all-gather.3.cloned.1.call-done) | copy-start | bytes 28311556
  150.0 8.2 %copy-start.3 = (bf16[2048,2048]{0,1:T(8,128)(2,1)S(1)}, bf16[2048,2048]{0,1:T(8,128)(2,1)}, u32[]{:S(2)}) copy-start(bf16[2048,2048]{0,1:T(8,128)(2,1)} %all-gather.5.cloned.1.call-done) | copy-start | bytes 25165828
  158.3 4.7 %copy-start.4 = (f32[768,1024]{1,0:T(8,128)}, f32[768,1024]{1,0:T(8,128)S(1)}, u32[]{:S(2)}) copy-start(f32[768,1024]{1,0:T(8,128)S(1)} %fusion.8) | copy-start | bytes 9437188
  166.5 3.7 %copy-start.6 = (bf16[768,1024]{1,0:T(8,128)(2,1)}, bf16[768,1024]{1,0:T(8,128)(2,1)S(1)}, u32[]{:S(2)}) copy-start(bf16[768,1024]{1,0:T(8,128)(2,1)S(1)} %multiply_convert_fusion.1) | copy-start | bytes 4718596
  179.9 8.2 %copy-start.5 = (f32[768,1024]{1,0:T(8,128)S(1)}, f32[768,1024]{1,0:T(8,128)}, u32[]{:S(2)}) copy-start(f32[768,1024]{1,0:T(8,128)} %copy-done.4) | copy-start | bytes 9437188
  179.9 132.7 %reduce-scatter.7.cloned.1.call-start = ((), (), s32[]{:S(2)}) async-start(), calls=%async_computation.5 | async-start | bytes 8912896
  216.2 1.0 copy-start
  216.2 1.2 copy-start.1
Sparse Core Ops, SparseCore 0:
  10.7 79.8 all-gather.4
  92.8 57.2 all-gather.2
  180.0 43.4 reduce-scatter.4
  226.8 85.7 reduce-scatter.6
where the time goes:
time: 323 us
  waiting for transfers between devices  230 us (71%)
  matrix products  39.4 us (12%)
  local copies, waits for them, and re-layouts  22 us (7%)
  other arithmetic  16.6 us (5%)
  between operations  13.9 us (4%)
    unnamed x5, waiting for transfers between devices  87.1 us
    all_gather x1, waiting for transfers between devices, gather_turned(): filled = lax.all_gather(both, axis, axis=0, tiled=True)  77.9 us
    all_gather x1, waiting for transfers between devices, in_one_piece(): lax.all_gather(both, axis, axis=dim, tiled=True)  59.5 us
    unnamed x21, local copies, waits for them, and re-layouts  20 us
    concatenate x1, other arithmetic, on_device(): jnp.concatenate((lax.dot_general(earlier_full, up_grad, contract_first, p...  8.54 us
    dot_general x1, matrix products, on_device(): lax.dot_general(earlier_full, up_grad, contract_first, preferred_element_...  8 us
    dot_general x1, matrix products, on_device(): lax.dot_general(cot_full, earlier_hidden, contract_first, preferred_eleme...  7.27 us
  transfers between devices with their start and end apart: 4, of which 4 were waited for; matrix products, arithmetic and copies ran while one was open for 13% of the time, Pallas kernels for 0%

commit v1 on v0

v1 whole, which is shorter than its diff:
```python
import jax
import jax.numpy as jnp
from jax import lax
from jax.experimental import pallas as pl
from jax.experimental.pallas import tpu as pltpu
from jax.sharding import PartitionSpec as P

contract_last = (((1,), (1,)), ((), ()))
contract_first = (((0,), (0,)), ((), ()))
bf16, f32 = jnp.bfloat16, jnp.float32
MESH = pl.DeviceIdType.MESH
SIDE = 4
ROWS, WIDTH, MODEL, HIDDEN = 768, 256, 2048, 1024
HALF = HIDDEN // 2


def around(k):
    return lax.rem(k + SIDE, SIDE)


class Place:
    def __init__(self):
        fs, tp = lax.axis_index("fs"), lax.axis_index("tp")
        self.z, self.x = fs // SIDE, lax.rem(fs, SIDE)
        self.y, self.core = tp // 2, lax.rem(tp, 2)

    def device(self, z=0, x=0, y=0, core=0):
        fs = around(self.z + z) * SIDE + around(self.x + x)
        tp = around(self.y + y) * 2 + lax.rem(self.core + core, 2)
        return (fs, tp)

    def neighbours(self):
        return [self.device(**{a: d}) for a in ("z", "x", "y") for d in (1, -1)] + [
            self.device(core=1)
        ]


class Ring:
    def __init__(self, place, axis, piece, sems, base):
        self.sems, self.base = sems, base
        at = getattr(place, axis)
        on, back = place.device(**{axis: 1}), place.device(**{axis: -1})
        before, after, across = around(at - 1), around(at + 1), around(at + 2)
        self.sent = [
            (piece(at, 0), on),
            (piece(at, 1), on),
            (piece(at, 1), back),
            (piece(at, 0), back),
            (piece(before, 0), on),
            (piece(after, 1), back),
        ]
        self.landed = [
            piece(before, 0),
            piece(before, 1),
            piece(after, 1),
            piece(after, 0),
            piece(across, 0),
            piece(across, 1),
        ]

    def copy(self, j, ref):
        send, receive = self.sems
        return pltpu.make_async_remote_copy(
            src_ref=ref,
            dst_ref=ref,
            send_sem=send.at[self.base + j],
            recv_sem=receive.at[self.base + j],
            device_id=self.sent[j][1],
            device_id_type=MESH,
        )

    def start(self, *which):
        for j in which:
            self.copy(j, self.sent[j][0]).start()

    def arrive(self, *which):
        for j in which:
            self.copy(j, self.landed[j]).wait_recv()

    def own(self):
        self.start(0, 2, 1, 3)

    def forward(self):
        self.arrive(0)
        self.start(4)
        self.arrive(2)
        self.start(5)

    def near(self):
        self.arrive(1, 3)

    def far(self):
        self.arrive(4, 5)

    def drain(self):
        for j in range(6):
            self.copy(j, self.sent[j][0]).wait_send()


class Partner:
    def __init__(self, place, block, sems, base):
        self.sems, self.base = sems, base
        self.device = place.device(core=1)
        steps = (0, -1, 1, 2)
        self.sent = [block(around(place.y + d), place.core) for d in steps]
        self.landed = [block(around(place.y + d), 1 - place.core) for d in steps]

    def copy(self, j, ref):
        send, receive = self.sems
        return pltpu.make_async_remote_copy(
            src_ref=ref,
            dst_ref=ref,
            send_sem=send.at[self.base + j],
            recv_sem=receive.at[self.base + j],
            device_id=self.device,
            device_id_type=MESH,
        )

    def start(self, *which):
        for j in which:
            self.copy(j, self.sent[j]).start()

    def finish(self):
        for j in range(4):
            self.copy(j, self.landed[j]).wait_recv()

    def drain(self):
        for j in range(4):
            self.copy(j, self.sent[j]).wait_send()


def gather_kernel(
    later_in, earlier_in, cot_in, up_in, down_in, act_out, up_out, down_out,
    act, up, down, load_sem, ring_send, ring_recv, pair_send, pair_recv,
):
    place = Place()
    barrier = pltpu.get_barrier_semaphore()
    for neighbour in place.neighbours():
        pl.semaphore_signal(barrier, inc=1, device_id=neighbour, device_id_type=MESH)

    def act_at(a, y, core, first, count):
        column = pl.multiple_of((y * 2 + core) * WIDTH, WIDTH)
        return act.at[a, pl.ds(first, count), pl.ds(column, WIDTH)]

    def down_at(h, s, first, count):
        return down.at[pl.ds(h * HALF + s * 256, 256), pl.ds(pl.multiple_of(first * 128, 128), count)]

    loads = []
    for a, ref in enumerate((earlier_in, cot_in, later_in)):
        loads.append((ref, act_at(a, place.y, place.core, 0, ROWS)))
    for h in range(2):
        loads.append((up_in.at[:, pl.ds(h * HALF, HALF)], up.at[h, place.z, place.x]))
    loads.append(
        (down_in, down.at[:, pl.ds(pl.multiple_of((place.z * SIDE + place.x) * 128, 128), 128)])
    )
    loads = [pltpu.make_async_copy(s, d, load_sem.at[i]) for i, (s, d) in enumerate(loads)]
    for load in loads:
        load.start()

    sems = (ring_send, ring_recv)
    rings = iter(range(0, 66, 6))
    rows = [
        Ring(place, "y", lambda k, s, a=a: act_at(a, k, place.core, s * 384, 384), sems, next(rings))
        for a in range(3)
    ]
    pairs = [
        Partner(place, lambda y, c, a=a: act_at(a, y, c, 0, ROWS), (pair_send, pair_recv), 4 * a)
        for a in range(3)
    ]
    first, second = [], []
    for h in range(2):
        first.append((
            Ring(place, "z", lambda k, s, h=h: up.at[h, k, place.x, pl.ds(s * 64, 64), :], sems, next(rings)),
            Ring(place, "x", lambda k, s, h=h: down_at(h, s, place.z * SIDE + k, 128), sems, next(rings)),
        ))
        second.append((
            Ring(place, "x", lambda k, s, h=h: up.at[h, :, k, pl.ds(s * 64, 64), :], sems, next(rings)),
            Ring(place, "z", lambda k, s, h=h: down_at(h, s, k * SIDE, 512), sems, next(rings)),
        ))

    def both(stage, name):
        for ring in stage:
            getattr(ring, name)()

    for load in loads:
        load.wait()
    pl.semaphore_wait(barrier, 7)

    both(first[0], "own")
    rows[0].own()
    pairs[0].start(0)
    both(first[0], "forward")
    both(first[1], "own")
    rows[0].forward()
    rows[1].own()
    pairs[1].start(0)
    both(first[0], "near")
    both(first[0], "far")
    both(second[0], "own")
    both(first[1], "forward")
    rows[0].near()
    pairs[0].start(1, 2)
    both(second[0], "forward")
    rows[0].far()
    pairs[0].start(3)
    rows[1].forward()
    rows[2].own()
    pairs[2].start(0)
    rows[1].near()
    pairs[1].start(1, 2)
    both(first[1], "near")
    both(first[1], "far")
    both(second[1], "own")
    both(second[0], "near")
    both(second[0], "far")
    rows[1].far()
    pairs[1].start(3)
    rows[2].forward()
    both(second[1], "forward")
    rows[2].near()
    pairs[2].start(1, 2)
    rows[2].far()
    pairs[2].start(3)
    both(second[1], "near")
    both(second[1], "far")
    for pair in pairs:
        pair.finish()
    stores = [(act.at[a], act_out.at[a]) for a in range(3)]
    stores += [(up.at[h], up_out.at[:, :, :, pl.ds(h * HALF, HALF)]) for h in range(2)]
    stores += [(down, down_out)]
    stores = [pltpu.make_async_copy(s, d, load_sem.at[i]) for i, (s, d) in enumerate(stores)]
    for store in stores:
        store.start()
    for ring in rows + [r for stage in first + second for r in stage]:
        ring.drain()
    for pair in pairs:
        pair.drain()
    for store in stores:
        store.wait()


def gather_all(later_input, earlier_input, cotangent, up_weight, down_weight):
    anywhere = pl.BlockSpec(memory_space=pl.ANY)
    act, up, down = pl.pallas_call(
        gather_kernel,
        out_shape=(
            jax.ShapeDtypeStruct((3, ROWS, MODEL), bf16),
            jax.ShapeDtypeStruct((SIDE, SIDE, 128, HIDDEN), bf16),
            jax.ShapeDtypeStruct((HIDDEN, MODEL), bf16),
        ),
        in_specs=[anywhere] * 5,
        out_specs=(anywhere,) * 3,
        scratch_shapes=[
            pltpu.VMEM((3, ROWS, MODEL), bf16),
            pltpu.VMEM((2, SIDE, SIDE, 128, HALF), bf16),
            pltpu.VMEM((HIDDEN, MODEL), bf16),
            pltpu.SemaphoreType.DMA((6,)),
            pltpu.SemaphoreType.DMA((66,)),
            pltpu.SemaphoreType.DMA((66,)),
            pltpu.SemaphoreType.DMA((12,)),
            pltpu.SemaphoreType.DMA((12,)),
        ],
        compiler_params=pltpu.CompilerParams(
            collective_id=0, has_side_effects=True, vmem_limit_bytes=60 * 2**20
        ),
    )(later_input, earlier_input, cotangent, up_weight, down_weight)
    return act[2], act[0], act[1], up.reshape(MODEL, HIDDEN), down


def side_by_side(arrays, axis, dim, along):
    both = jnp.concatenate(arrays, axis=along)
    filled, at, outs = (lax.psum_scatter(both, axis, scatter_dimension=dim, tiled=True), 0, [])
    for a in arrays:
        outs.append(lax.slice_in_dim(filled, at, at + a.shape[along], axis=along))
        at += a.shape[along]
    return tuple(outs)


def on_device(
    later_input, earlier_input, cotangent, up_weight, down_weight, up_running, down_running
):
    rows = later_input.shape[0]
    factor = float(rows * lax.axis_size("fs")) ** (-0.5)
    columns = up_weight.shape[1]
    later_full, earlier_full, cot_full, up_whole, down_whole = gather_all(
        later_input, earlier_input, cotangent, up_weight, down_weight
    )
    later_up = jnp.dot(later_full, up_whole, preferred_element_type=f32)
    earlier_up = jnp.dot(earlier_full, up_whole, preferred_element_type=f32)
    later_hidden = jnp.square(jax.nn.relu(later_up)).astype(bf16)
    out_part = jnp.dot(later_hidden, down_whole, preferred_element_type=f32)
    hidden_grad = lax.dot_general(cot_full, down_whole, contract_last, preferred_element_type=f32)
    up_grad = (2.0 * jax.nn.relu(earlier_up) * hidden_grad).astype(bf16)
    back_part = lax.dot_general(up_grad, up_whole, contract_last, preferred_element_type=f32)
    later_preact = later_up.astype(bf16)
    earlier_hidden = jnp.square(jax.nn.relu(earlier_up)).astype(bf16)
    out_sum, back_sum = tuple(
        (
            part.astype(f32)
            for part in side_by_side((out_part.astype(bf16), back_part.astype(bf16)), "tp", 1, 0)
        )
    )
    summed = lax.psum_scatter(
        jnp.concatenate(
            (
                lax.dot_general(earlier_full, up_grad, contract_first, preferred_element_type=f32),
                lax.dot_general(cot_full, earlier_hidden, contract_first, preferred_element_type=f32),
            ),
            axis=1,
        ).astype(bf16),
        "fs",
        scatter_dimension=0,
        tiled=True,
    ).astype(f32)
    return (
        out_sum.astype(bf16),
        later_preact,
        back_sum.astype(bf16),
        up_running + summed[:, :columns] * factor,
        down_running + summed[:, columns:] * factor,
    )


def solution(mesh):
    in_specs = (
        P("fs", "tp"),
        P("fs", "tp"),
        P("fs", "tp"),
        P("fs", "tp"),
        P("tp", "fs"),
        P("fs", "tp"),
        P("fs", "tp"),
    )
    out_specs = (P("fs", "tp"),) * 5
    return jax.shard_map(
        on_device, mesh=mesh, in_specs=in_specs, out_specs=out_specs, check_vma=False
    )
```

time: 323 us -> 233 us (0.72)
  waiting for transfers between devices: 230 us -> 90.2 us
  Pallas kernels: 0 us -> 59.2 us
  other arithmetic: 16.6 us -> 12.5 us
    all_gather x2 -> x0, waiting for transfers between devices: 137 us -> none  [the longest x1 77.9 us: gather_turned(): filled = lax.all_gather(both, axis, axis=0, tiled=True)]
    pallas_call x0 -> x1, Pallas kernels: none -> 59.2 us  [gather_all(): pl.pallas_call(gather_kernel, out_shape=(jax.ShapeDtypeStruct((3, ROWS, M...]
    concatenate x2 -> x0, other arithmetic: 4.11 us -> none  [the longest x1 2.32 us: in_one_piece(): both = jnp.concatenate(arrays, axis=along)]
    reduce_scatter x1, waiting for transfers between devices: 5.87 us -> 2.55 us  [side_by_side(): lax.psum_scatter(both, axis, scatter_dimension=dim, tiled=True)]
    unnamed x21 -> x18, local copies, waits for them, and re-layouts: 20 us -> 17.8 us
    unnamed x5 -> x3, waiting for transfers between devices: 87.1 us -> 87.6 us
  transfers between devices with their start and end apart: 4 -> 2, of which waited for: 4 -> 2; matrix products, arithmetic and copies ran while one was open for 13% -> 16% of each run, Pallas kernels for 0% -> 0%
where the time goes in v1:
time: 233 us
  waiting for transfers between devices  90.2 us (39%)
  Pallas kernels  59.2 us (25%)
  matrix products  36.5 us (16%)
  local copies, waits for them, and re-layouts  19.8 us (8%)
  between operations  14.2 us (6%)
  other arithmetic  12.5 us (5%)
    unnamed x3, waiting for transfers between devices  87.6 us
    pallas_call x1, Pallas kernels, gather_all(): pl.pallas_call(gather_kernel, out_shape=(jax.ShapeDtypeStruct((3, ROWS, M...  59.2 us
    unnamed x18, local copies, waits for them, and re-layouts  17.8 us
    concatenate x1, other arithmetic, on_device(): jnp.concatenate((lax.dot_general(earlier_full, up_grad, contract_first, p...  8.54 us
    dot_general x1, matrix products, on_device(): lax.dot_general(earlier_full, up_grad, contract_first, preferred_element_...  7.84 us
    dot_general x1, matrix products, on_device(): lax.dot_general(cot_full, earlier_hidden, contract_first, preferred_eleme...  6.94 us
    dot_general x1, matrix products, on_device(): earlier_up = jnp.dot(earlier_full, up_whole, preferred_element_type=f32)  6.29 us
  transfers between devices with their start and end apart: 2, of which 2 were waited for; matrix products, arithmetic and copies ran while one was open for 16% of the time, Pallas kernels for 0%

profile of v1, /device:TPU:0, one launch (start us, length us, event | category | flops | bytes accessed | tf_op | source)
XLA Modules:
  0.0 232.7 jit_solution(13745036002640648694)
XLA Ops:
  7.2 59.2 %shard_map.110 = (bf16[3,768,2048]{2,1,0:T(8,128)(2,1)}, bf16[4,4,128,1024]{3,2,1,0:T(8,128)(2,1)}, bf16[1024,2048]{1,0:T(8,128)(2,1)}) custom-call(bf16[768,256]{1,0:T(8,128)(2,1)} %later_in.1, bf16[768,256]{1,0:T(8,128)(2,1)} %earlier_in.1, bf16[768,256]{1,0:T(8,128)(2,1)} %cot_in.1, bf16[128,1024]{1,0:T(8,128)(2,1)} %up_in.1, bf16[1024,128]{1,0:T(8,128)(2,1)} %down_in.1), custom_call_target="tpu_custom_call" | custom-call | tf_op jit(solution)/shard_map/pallas_call | solution.py:244
  66.4 6.3 %fusion.4 = f32[768,1024]{1,0:T(8,128)S(1)} fusion(bf16[2048,1024]{1,0:T(8,128)(2,1)} %bitcast.26, bf16[3,768,2048]{2,1,0:T(8,128)(2,1)} %get-tuple-element.8), kind=kOutput, calls=%fused_computation.10 | convolution fusion | flops 3221225472 | bytes 10485760 | tf_op jit(solution)/shard_map/dot_general | solution.py:289
  72.7 0.7 copy-done.4
  73.4 4.6 %fusion.22 = (bf16[768,1024]{1,0:T(8,128)(2,1)}, f32[768,1024]{1,0:T(8,128)S(1)}) fusion(bf16[2048,1024]{1,0:T(8,128)(2,1)S(1)} %bitcast.27, bf16[3,768,2048]{2,1,0:T(8,128)(2,1)S(1)} %copy-done.2), kind=kOutput, calls=%fused_computation.31 | convolution fusion | flops 3222011904 | bytes 12058624 | tf_op jit(solution)/shard_map/dot_general | solution.py:288
  78.0 3.5 %multiply_convert_fusion.1 = bf16[768,1024]{1,0:T(8,128)(2,1)S(1)} fusion(f32[768,1024]{1,0:T(8,128)S(1)} %fusion.4, bf16[1024,2048]{1,0:T(8,128)(2,1)S(1)} %copy-done.3, bf16[3,768,2048]{2,1,0:T(8,128)(2,1)S(1)} %copy-done.2), kind=kOutput, calls=%fused_computation.15 | convolution fusion | flops 3224371200 | bytes 12058624 | tf_op jit(solution)/shard_map/dot_general | solution.py:292
  81.5 3.7 %convolution_convert_fusion.2 = bf16[768,2048]{1,0:T(8,128)(2,1)S(1)} fusion(bf16[768,1024]{1,0:T(8,128)(2,1)S(1)} %multiply_convert_fusion.1, bf16[2048,1024]{1,0:T(8,128)(2,1)S(1)} %bitcast.28), kind=kOutput, calls=%fused_computation.4 | convolution fusion | flops 3222798336 | bytes 8912896 | tf_op jit(solution)/shard_map/dot_general | solution.py:294
  85.2 3.7 %convolution_convert_fusion.3 = bf16[768,2048]{1,0:T(8,128)(2,1)S(1)} fusion(bf16[1024,2048]{1,0:T(8,128)(2,1)S(1)} %copy-done.3, f32[768,1024]{1,0:T(8,128)S(1)} %get-tuple-element.26), kind=kOutput, calls=%fused_computation.5 | convolution fusion | flops 3225157632 | bytes 10485760 | tf_op jit(solution)/shard_map/dot_general | solution.py:291
  88.9 3.8 %pad_maximum_fusion.1 = bf16[1536,2048]{1,0:T(8,128)(2,1)} fusion(bf16[768,2048]{1,0:T(8,128)(2,1)S(1)} %convolution_convert_fusion.2, bf16[768,2048]{1,0:T(8,128)(2,1)S(1)} %convolution_convert_fusion.3), kind=kLoop, calls=%fused_computation.1 | loop fusion | flops 12582912 | bytes 12582912 | tf_op jit(solution)/shard_map/concatenate | solution.py:271
  92.7 0.2 reduce-scatter.7.cloned.1.call-start
  93.0 7.8 %convolution_convert_fusion.1 = bf16[2048,1024]{0,1:T(8,128)(2,1)} fusion(bf16[768,1024]{1,0:T(8,128)(2,1)} %copy-done.5, bf16[3,768,2048]{2,1,0:T(8,128)(2,1)} %get-tuple-element.8), kind=kOutput, calls=%fused_computation.3 | convolution fusion | flops 3223322624 | bytes 8912896 | tf_op jit(solution)/shard_map/dot_general | solution.py:306
  100.8 6.9 %convolution_convert_fusion = bf16[2048,1024]{0,1:T(8,128)(2,1)} fusion(bf16[3,768,2048]{2,1,0:T(8,128)(2,1)} %get-tuple-element.8, f32[768,1024]{1,0:T(8,128)S(1)} %fusion.4), kind=kOutput, calls=%fused_computation.2 | convolution fusion | flops 3225681920 | bytes 10485760 | tf_op jit(solution)/shard_map/dot_general | solution.py:307
  107.7 8.5 %pad_maximum_fusion = bf16[2048,2048]{0,1:T(8,128)(2,1)} fusion(bf16[2048,1024]{0,1:T(8,128)(2,1)} %convolution_convert_fusion, bf16[2048,1024]{0,1:T(8,128)(2,1)} %convolution_convert_fusion.1), kind=kLoop, calls=%fused_computation | loop fusion | flops 16777216 | bytes 16777216 | tf_op jit(solution)/shard_map/concatenate | solution.py:304
  116.3 12.4 %copy.20 = bf16[2048,2048]{1,0:T(8,128)(2,1)} copy(bf16[2048,2048]{0,1:T(8,128)(2,1)} %pad_maximum_fusion) | data formatting | bytes 16777216
  128.7 1.0 copy-done
  129.7 0.2 copy.17
  129.9 0.2 copy.16
  130.1 2.6 %reduce-scatter.5.cloned.1.call-done = bf16[1536,256]{1,0:T(8,128)(2,1)} async-done(((bf16[1536,2048]{1,0:T(8,128)(2,1)}), bf16[1536,256]{1,0:T(8,128)(2,1)}) %reduce-scatter.5.cloned.1.call-update) | async-done | bytes 786448 | tf_op jit(solution)/shard_map/reduce_scatter | solution.py:272
  132.7 2.0 fusion.21
  134.7 87.6 %reduce-scatter.7.cloned.1.call-done = bf16[128,2048]{1,0:T(8,128)(2,1)} async-done(((bf16[2048,2048]{1,0:T(8,128)(2,1)}), bf16[128,2048]{1,0:T(8,128)(2,1)}) %reduce-scatter.7.cloned.1.call-update) | async-done | bytes 524304
  222.3 1.3 copy.21
  223.6 0.1 convert_element_type.32
  223.7 0.1 fusion.17
  223.8 1.0 copy.18
  224.8 1.0 copy.19
  (13 shorter events, 0.1 us)
Async XLA Ops:
  7.2 125.5 %reduce-scatter.5.cloned.1.call-start = ((), (), s32[]{:S(2)}) async-start(), calls=%async_computation.2 | async-start | bytes 7077888 | tf_op jit(solution)/shard_map/reduce_scatter | solution.py:272
  66.4 6.3 %copy-start.2 = (bf16[3,768,2048]{2,1,0:T(8,128)(2,1)S(1)}, bf16[3,768,2048]{2,1,0:T(8,128)(2,1)}, u32[]{:S(2)}) copy-start(bf16[3,768,2048]{2,1,0:T(8,128)(2,1)} %get-tuple-element.8) | copy-start | bytes 28311556
  66.4 7.0 %copy-start.4 = (bf16[4,4,128,1024]{3,2,1,0:T(8,128)(2,1)S(1)}, bf16[4,4,128,1024]{3,2,1,0:T(8,128)(2,1)}, u32[]{:S(2)}) copy-start(bf16[4,4,128,1024]{3,2,1,0:T(8,128)(2,1)} %get-tuple-element.9) | copy-start | bytes 12582916
  73.4 4.6 %copy-start.3 = (bf16[1024,2048]{1,0:T(8,128)(2,1)S(1)}, bf16[1024,2048]{1,0:T(8,128)(2,1)}, u32[]{:S(2)}) copy-start(bf16[1024,2048]{1,0:T(8,128)(2,1)} %get-tuple-element.10) | copy-start | bytes 12582916
  81.5 3.7 %copy-start.5 = (bf16[768,1024]{1,0:T(8,128)(2,1)}, bf16[768,1024]{1,0:T(8,128)(2,1)S(1)}, u32[]{:S(2)}) copy-start(bf16[768,1024]{1,0:T(8,128)(2,1)S(1)} %multiply_convert_fusion.1) | copy-start | bytes 4718596
  92.7 129.6 %reduce-scatter.7.cloned.1.call-start = ((), (), s32[]{:S(2)}) async-start(), calls=%async_computation.3 | async-start | bytes 8912896
  128.7 1.1 copy-start
  128.7 1.3 copy-start.1
Sparse Core Ops, SparseCore 0:
  92.9 39.7 reduce-scatter.4
  136.1 86.1 reduce-scatter.6

commit v2 on v1

--- a/solution.py
+++ b/solution.py
@@ -12,6 +12,7 @@
 SIDE = 4
 ROWS, WIDTH, MODEL, HIDDEN = 768, 256, 2048, 1024
 HALF = HIDDEN // 2
+STRIP = ROWS // 2
 
 
 def around(k):
@@ -129,9 +130,82 @@
             self.copy(j, self.sent[j]).wait_send()
 
 
-def gather_kernel(
-    later_in, earlier_in, cot_in, up_in, down_in, act_out, up_out, down_out,
-    act, up, down, load_sem, ring_send, ring_recv, pair_send, pair_recv,
+class RingSum:
+    def __init__(self, place, axis, block, far, near, sems, base):
+        self.sems, self.base = sems, base
+        at = getattr(place, axis)
+        on, back = place.device(**{axis: 1}), place.device(**{axis: -1})
+        before, after, across = around(at - 1), around(at + 1), around(at + 2)
+        self.mine = [block(at, s) for s in range(2)]
+        self.far, self.near = far, near
+        self.sent = [
+            (block(across, 0), far(0), on),
+            (block(across, 1), far(1), back),
+            (block(after, 1), near(0, 1), on),
+            (block(before, 0), near(1, 0), back),
+            (block(after, 0), near(0, 0), on),
+            (block(before, 1), near(1, 1), back),
+        ]
+
+    def copy(self, j):
+        send, receive = self.sems
+        src, dst, device = self.sent[j]
+        return pltpu.make_async_remote_copy(
+            src_ref=src,
+            dst_ref=dst,
+            send_sem=send.at[self.base + j],
+            recv_sem=receive.at[self.base + j],
+            device_id=device,
+            device_id_type=MESH,
+        )
+
+    def begin(self):
+        for j in (0, 1, 2, 3):
+            self.copy(j).start()
+
+    def middle(self):
+        for j in range(2):
+            self.copy(j).wait_recv()
+            ref = self.sent[4 + j][0]
+            ref[...] = (ref[...].astype(f32) + self.far(j)[...].astype(f32)).astype(bf16)
+            self.copy(4 + j).start()
+
+    def total(self, s):
+        return (
+            self.mine[s][...].astype(f32)
+            + self.near(0, s)[...].astype(f32)
+            + self.near(1, s)[...].astype(f32)
+        )
+
+    def arrive(self):
+        for j in (2, 3, 4, 5):
+            self.copy(j).wait_recv()
+
+    def finish(self):
+        self.arrive()
+        for s in range(2):
+            self.mine[s][...] = self.total(s).astype(bf16)
+
+    def drain(self):
+        for j in range(6):
+            self.copy(j).wait_send()
+
+
+def dot(a, b):
+    return jnp.dot(a, b, preferred_element_type=f32)
+
+
+def dot_turned(a, b):
+    return lax.dot_general(a, b, contract_last, preferred_element_type=f32)
+
+
+def layer_kernel(
+    factor,
+    later_in, earlier_in, cot_in, up_in, down_in, up_run_in, down_run_in,
+    out_hbm, pre_hbm, back_hbm, up_run_hbm, down_run_hbm,
+    act, turned, up, down, first_up, hidden, grad, pre, part, other, run, up_sum, down_sum,
+    far_row, near_row, far_one, near_one, far_two, near_two,
+    load_sem, ring_send, ring_recv, pair_send, pair_recv, sum_send, sum_recv,
 ):
     place = Place()
     barrier = pltpu.get_barrier_semaphore()
@@ -153,6 +227,7 @@
     loads.append(
         (down_in, down.at[:, pl.ds(pl.multiple_of((place.z * SIDE + place.x) * 128, 128), 128)])
     )
+    loads += [(up_run_in, run.at[0]), (down_run_in, run.at[1])]
     loads = [pltpu.make_async_copy(s, d, load_sem.at[i]) for i, (s, d) in enumerate(loads)]
     for load in loads:
         load.start()
@@ -178,9 +253,126 @@
             Ring(place, "z", lambda k, s, h=h: down_at(h, s, k * SIDE, 512), sems, next(rings)),
         ))
 
+    sems = (sum_send, sum_recv)
+    sums = iter(range(0, 60, 6))
+    row_sums = [
+        RingSum(
+            place, "y", lambda k, s, a=a: part.at[a, place.core, k, pl.ds(s * 384, 384), :],
+            lambda d, a=a: far_row.at[a, d], lambda d, s, a=a: near_row.at[a, d, s], sems, next(sums),
+        )
+        for a in range(2)
+    ]
+    up_one, up_two, down_one, down_two = [], [], [], []
+    for h in range(2):
+        up_one.append(RingSum(
+            place, "x", lambda k, s, h=h: up_sum.at[h, :, k, pl.ds(s * 64, 64), :],
+            lambda d, h=h: far_one.at[0, h, d], lambda d, s, h=h: near_one.at[0, h, d, s], sems, next(sums),
+        ))
+        down_one.append(RingSum(
+            place, "z", lambda k, s, h=h: down_sum.at[h, k, :, pl.ds(s * 64, 64), :],
+            lambda d, h=h: far_one.at[1, h, d], lambda d, s, h=h: near_one.at[1, h, d, s], sems, next(sums),
+        ))
+        up_two.append(RingSum(
+            place, "z", lambda k, s, h=h: up_sum.at[h, k, place.x, pl.ds(s * 64, 64), :],
+            lambda d, h=h: far_two.at[0, h, d], lambda d, s, h=h: near_two.at[0, h, d, s], sems, next(sums),
+        ))
+        down_two.append(RingSum(
+            place, "x", lambda k, s, h=h: down_sum.at[h, place.z, k, pl.ds(s * 64, 64), :],
+            lambda d, h=h: far_two.at[1, h, d], lambda d, s, h=h: near_two.at[1, h, d, s], sems, next(sums),
+        ))
+
+    def swap(a):
+        return pltpu.make_async_remote_copy(
+            src_ref=part.at[a, 1 - place.core],
+            dst_ref=other.at[a],
+            send_sem=pair_send.at[12 + a],
+            recv_sem=pair_recv.at[12 + a],
+            device_id=place.device(core=1),
+            device_id_type=MESH,
+        )
+
     def both(stage, name):
         for ring in stage:
             getattr(ring, name)()
+
+    def strip(m):
+        return pl.ds(pl.multiple_of(m * STRIP, STRIP), STRIP)
+
+    def columns(h):
+        return pl.ds(h * HALF, HALF)
+
+    def turn(a):
+        @pl.loop(0, 8)
+        def _(n):
+            block = pl.ds(pl.multiple_of(n * 256, 256), 256)
+            turned[a, block, :] = act[a, :, block].T
+
+    def up_of(h):
+        return up[h].reshape(MODEL, HALF)
+
+    def earlier_up(h):
+        @pl.loop(0, 2)
+        def _(m):
+            value = jnp.maximum(dot(act[0, strip(m), :], up_of(h)), 0.0)
+            first_up[strip(m), :] = value
+            hidden[strip(m), columns(h)] = jnp.square(value).astype(bf16)
+
+    def hidden_grad(h):
+        @pl.loop(0, 2)
+        def _(m):
+            value = dot_turned(act[1, strip(m), :], down[columns(h), :])
+            grad[strip(m), columns(h)] = (2.0 * first_up[strip(m), :] * value).astype(bf16)
+
+    def weight_grad(a, source, target, h):
+        @pl.loop(0, 4)
+        def _(n):
+            block = pl.ds(pl.multiple_of(n * 512, 512), 512)
+            value = dot(turned[a, block, :], source[:, columns(h)])
+            target[h, n] = value.astype(bf16).reshape(SIDE, 128, HALF)
+
+    def later_up(h):
+        @pl.loop(0, 2)
+        def _(m):
+            value = dot(act[2, strip(m), :], up_of(h))
+            pre[strip(m), columns(h)] = value.astype(bf16)
+            hidden[strip(m), columns(h)] = jnp.square(jnp.maximum(value, 0.0)).astype(bf16)
+
+    def keep(a, n, m, value):
+        value = value.astype(bf16)
+        part[a, 0, n, strip(m), :] = value[:, :WIDTH]
+        part[a, 1, n, strip(m), :] = value[:, WIDTH:]
+
+    def later_out():
+        @pl.loop(0, 4)
+        def _(n):
+            block = pl.ds(pl.multiple_of(n * 512, 512), 512)
+
+            @pl.loop(0, 2)
+            def _(m):
+                keep(0, n, m, dot(hidden[strip(m), :], down[:, block]))
+
+    def input_grad():
+        @pl.loop(0, 4)
+        def _(n):
+            @pl.loop(0, 2)
+            def _(m):
+                weight = jnp.concatenate([up[h, n].reshape(512, HALF) for h in range(2)], axis=1)
+                keep(1, n, m, dot_turned(grad[strip(m), :], weight))
+
+    def join(a):
+        swap(a).wait_recv()
+
+        @pl.loop(0, 4)
+        def _(k):
+            part[a, place.core, k] = (
+                part[a, place.core, k].astype(f32) + other[a, k].astype(f32)
+            ).astype(bf16)
+
+    def add_running(w, ring, h):
+        ring.arrive()
+        for s in range(2):
+            at = run.at[w, pl.ds(s * 64, 64), columns(h)]
+            at[...] = at[...] + ring.total(s) * factor
 
     for load in loads:
         load.wait()
@@ -203,6 +395,8 @@
     both(second[0], "forward")
     rows[0].far()
     pairs[0].start(3)
+    pairs[0].finish()
+    turn(0)
     rows[1].forward()
     rows[2].own()
     pairs[2].start(0)
@@ -213,112 +407,134 @@
     both(second[1], "own")
     both(second[0], "near")
     both(second[0], "far")
+    earlier_up(0)
     rows[1].far()
     pairs[1].start(3)
     rows[2].forward()
+    pairs[1].finish()
+    turn(1)
     both(second[1], "forward")
+    weight_grad(1, hidden, down_sum, 0)
+    down_one[0].begin()
     rows[2].near()
     pairs[2].start(1, 2)
+    hidden_grad(0)
+    weight_grad(0, grad, up_sum, 0)
+    up_one[0].begin()
     rows[2].far()
     pairs[2].start(3)
     both(second[1], "near")
     both(second[1], "far")
-    for pair in pairs:
-        pair.finish()
-    stores = [(act.at[a], act_out.at[a]) for a in range(3)]
-    stores += [(up.at[h], up_out.at[:, :, :, pl.ds(h * HALF, HALF)]) for h in range(2)]
-    stores += [(down, down_out)]
-    stores = [pltpu.make_async_copy(s, d, load_sem.at[i]) for i, (s, d) in enumerate(stores)]
-    for store in stores:
-        store.start()
+    earlier_up(1)
+    hidden_grad(1)
+    weight_grad(1, hidden, down_sum, 1)
+    down_one[0].middle()
+    up_one[0].middle()
+    down_one[1].begin()
+    weight_grad(0, grad, up_sum, 1)
+    up_one[1].begin()
+    input_grad()
+    swap(1).start()
+    pairs[2].finish()
+    later_up(0)
+    later_up(1)
+    keep_pre = pltpu.make_async_copy(pre, pre_hbm, load_sem.at[0])
+    keep_pre.start()
+    join(1)
+    row_sums[1].begin()
+    down_one[0].finish()
+    down_two[0].begin()
+    up_one[0].finish()
+    up_two[0].begin()
+    later_out()
+    swap(0).start()
+    down_one[1].middle()
+    up_one[1].middle()
+    join(0)
+    row_sums[1].middle()
+    row_sums[0].begin()
+    down_two[0].middle()
+    up_two[0].middle()
+    down_one[1].finish()
+    down_two[1].begin()
+    up_one[1].finish()
+    up_two[1].begin()
+    row_sums[0].middle()
+    row_sums[1].finish()
+    own = [part.at[a, place.core, place.y] for a in range(2)]
+    keep_back = pltpu.make_async_copy(own[1], back_hbm, load_sem.at[1])
+    keep_back.start()
+    add_running(1, down_two[0], 0)
+    add_running(0, up_two[0], 0)
+    down_two[1].middle()
+    up_two[1].middle()
+    row_sums[0].finish()
+    keep_out = pltpu.make_async_copy(own[0], out_hbm, load_sem.at[2])
+    keep_out.start()
+    add_running(1, down_two[1], 1)
+    keep_down = pltpu.make_async_copy(run.at[1], down_run_hbm, load_sem.at[3])
+    keep_down.start()
+    add_running(0, up_two[1], 1)
+    keep_up = pltpu.make_async_copy(run.at[0], up_run_hbm, load_sem.at[4])
+    keep_up.start()
     for ring in rows + [r for stage in first + second for r in stage]:
         ring.drain()
     for pair in pairs:
         pair.drain()
-    for store in stores:
+    for ring in row_sums + up_one + up_two + down_one + down_two:
+        ring.drain()
+    for a in range(2):
+        swap(a).wait_send()
+    for store in (keep_pre, keep_back, keep_out, keep_down, keep_up):
         store.wait()
 
 
-def gather_all(later_input, earlier_input, cotangent, up_weight, down_weight):
+def on_device(*arrays):
+    factor = float(ROWS * 16) ** (-0.5)
     anywhere = pl.BlockSpec(memory_space=pl.ANY)
-    act, up, down = pl.pallas_call(
-        gather_kernel,
+    return pl.pallas_call(
+        lambda *refs: layer_kernel(factor, *refs),
         out_shape=(
-            jax.ShapeDtypeStruct((3, ROWS, MODEL), bf16),
-            jax.ShapeDtypeStruct((SIDE, SIDE, 128, HIDDEN), bf16),
-            jax.ShapeDtypeStruct((HIDDEN, MODEL), bf16),
+            jax.ShapeDtypeStruct((ROWS, WIDTH), bf16),
+            jax.ShapeDtypeStruct((ROWS, HIDDEN), bf16),
+            jax.ShapeDtypeStruct((ROWS, WIDTH), bf16),
+            jax.ShapeDtypeStruct((128, HIDDEN), f32),
+            jax.ShapeDtypeStruct((128, HIDDEN), f32),
         ),
-        in_specs=[anywhere] * 5,
-        out_specs=(anywhere,) * 3,
+        in_specs=[anywhere] * 7,
+        out_specs=(anywhere,) * 5,
         scratch_shapes=[
             pltpu.VMEM((3, ROWS, MODEL), bf16),
+            pltpu.VMEM((2, MODEL, ROWS), bf16),
             pltpu.VMEM((2, SIDE, SIDE, 128, HALF), bf16),
             pltpu.VMEM((HIDDEN, MODEL), bf16),
-            pltpu.SemaphoreType.DMA((6,)),
+            pltpu.VMEM((ROWS, HALF), f32),
+            pltpu.VMEM((ROWS, HIDDEN), bf16),
+            pltpu.VMEM((ROWS, HIDDEN), bf16),
+            pltpu.VMEM((ROWS, HIDDEN), bf16),
+            pltpu.VMEM((2, 2, SIDE, ROWS, WIDTH), bf16),
+            pltpu.VMEM((2, SIDE, ROWS, WIDTH), bf16),
+            pltpu.VMEM((2, 128, HIDDEN), f32),
+            pltpu.VMEM((2, SIDE, SIDE, 128, HALF), bf16),
+            pltpu.VMEM((2, SIDE, SIDE, 128, HALF), bf16),
+            pltpu.VMEM((2, 2, STRIP, WIDTH), bf16),
+            pltpu.VMEM((2, 2, 2, STRIP, WIDTH), bf16),
+            pltpu.VMEM((2, 2, 2, SIDE, 64, HALF), bf16),
+            pltpu.VMEM((2, 2, 2, 2, SIDE, 64, HALF), bf16),
+            pltpu.VMEM((2, 2, 2, 64, HALF), bf16),
+            pltpu.VMEM((2, 2, 2, 2, 64, HALF), bf16),
+            pltpu.SemaphoreType.DMA((8,)),
             pltpu.SemaphoreType.DMA((66,)),
             pltpu.SemaphoreType.DMA((66,)),
-            pltpu.SemaphoreType.DMA((12,)),
-            pltpu.SemaphoreType.DMA((12,)),
+            pltpu.SemaphoreType.DMA((14,)),
+            pltpu.SemaphoreType.DMA((14,)),
+            pltpu.SemaphoreType.DMA((60,)),
+            pltpu.SemaphoreType.DMA((60,)),
         ],
         compiler_params=pltpu.CompilerParams(
-            collective_id=0, has_side_effects=True, vmem_limit_bytes=60 * 2**20
+            collective_id=0, has_side_effects=True, vmem_limit_bytes=63 * 2**20
         ),
-    )(later_input, earlier_input, cotangent, up_weight, down_weight)
-    return act[2], act[0], act[1], up.reshape(MODEL, HIDDEN), down
-
-
-def side_by_side(arrays, axis, dim, along):
-    both = jnp.concatenate(arrays, axis=along)
-    filled, at, outs = (lax.psum_scatter(both, axis, scatter_dimension=dim, tiled=True), 0, [])
-    for a in arrays:
-        outs.append(lax.slice_in_dim(filled, at, at + a.shape[along], axis=along))
-        at += a.shape[along]
-    return tuple(outs)
-
-
-def on_device(
-    later_input, earlier_input, cotangent, up_weight, down_weight, up_running, down_running
-):
-    rows = later_input.shape[0]
-    factor = float(rows * lax.axis_size("fs")) ** (-0.5)
-    columns = up_weight.shape[1]
-    later_full, earlier_full, cot_full, up_whole, down_whole = gather_all(
-        later_input, earlier_input, cotangent, up_weight, down_weight
-    )
-    later_up = jnp.dot(later_full, up_whole, preferred_element_type=f32)
-    earlier_up = jnp.dot(earlier_full, up_whole, preferred_element_type=f32)
-    later_hidden = jnp.square(jax.nn.relu(later_up)).astype(bf16)
-    out_part = jnp.dot(later_hidden, down_whole, preferred_element_type=f32)
-    hidden_grad = lax.dot_general(cot_full, down_whole, contract_last, preferred_element_type=f32)
-    up_grad = (2.0 * jax.nn.relu(earlier_up) * hidden_grad).astype(bf16)
-    back_part = lax.dot_general(up_grad, up_whole, contract_last, preferred_element_type=f32)
-    later_preact = later_up.astype(bf16)
-    earlier_hidden = jnp.square(jax.nn.relu(earlier_up)).astype(bf16)
-    out_sum, back_sum = tuple(
-        (
-            part.astype(f32)
-            for part in side_by_side((out_part.astype(bf16), back_part.astype(bf16)), "tp", 1, 0)
-        )
-    )
-    summed = lax.psum_scatter(
-        jnp.concatenate(
-            (
-                lax.dot_general(earlier_full, up_grad, contract_first, preferred_element_type=f32),
-                lax.dot_general(cot_full, earlier_hidden, contract_first, preferred_element_type=f32),
-            ),
-            axis=1,
-        ).astype(bf16),
-        "fs",
-        scatter_dimension=0,
-        tiled=True,
-    ).astype(f32)
-    return (
-        out_sum.astype(bf16),
-        later_preact,
-        back_sum.astype(bf16),
-        up_running + summed[:, :columns] * factor,
-        down_running + summed[:, columns:] * factor,
-    )
+    )(*arrays)
 
 
 def solution(mesh):

time: 233 us -> 111 us (0.48)
  waiting for transfers between devices: 90.2 us -> 0 us
  Pallas kernels: 59.2 us -> 102 us
  matrix products: 36.5 us -> 0 us
  between operations: 14.2 us -> 0.65 us
  local copies, waits for them, and re-layouts: 19.8 us -> 6.86 us
  other arithmetic: 12.5 us -> 0 us
    unnamed x3 -> x0, waiting for transfers between devices: 87.6 us -> none
    pallas_call x1, Pallas kernels: 59.2 us -> 102 us  [on_device(): pl.pallas_call(lambda *refs: layer_kernel(factor, *refs), out_shape=(jax....]
    dot_general x7 -> x0, matrix products: 36.5 us -> none  [the longest x1 7.84 us: on_device(): lax.dot_general(earlier_full, up_grad, contract_first, preferred_element_...]
    concatenate x2 -> x0, other arithmetic: 12.3 us -> none  [the longest x1 8.54 us: on_device(): jnp.concatenate((lax.dot_general(earlier_full, up_grad, contract_first, p...]
    unnamed x18 -> x11, local copies, waits for them, and re-layouts: 17.8 us -> 6.86 us
    reduce_scatter x1 -> x0, waiting for transfers between devices: 2.55 us -> none  [side_by_side(): lax.psum_scatter(both, axis, scatter_dimension=dim, tiled=True)]
  transfers between devices with their start and end apart: 2 -> 0, of which waited for: 2 -> 0; matrix products, arithmetic and copies ran while one was open for 16% -> 0% of each run, Pallas kernels for 0% -> 0%
where the time goes in v2:
time: 111 us; the launch traced here: 110 us
  Pallas kernels  102 us (92%)
  local copies, waits for them, and re-layouts  6.86 us (6%)
    pallas_call x1, Pallas kernels, on_device(): pl.pallas_call(lambda *refs: layer_kernel(factor, *refs), out_shape=(jax....  102 us
    unnamed x11, local copies, waits for them, and re-layouts  6.86 us

profile of v2, /device:TPU:0, one launch (start us, length us, event | category | flops | bytes accessed | tf_op | source)
XLA Modules:
  0.0 109.8 jit_solution(14824312244735409121)
XLA Ops:
  0.6 102.3 %shard_map.110 = (bf16[768,256]{1,0:T(8,128)(2,1)}, bf16[768,1024]{1,0:T(8,128)(2,1)}, bf16[768,256]{1,0:T(8,128)(2,1)}, f32[128,1024]{1,0:T(8,128)}, f32[128,1024]{1,0:T(8,128)}) custom-call(bf16[768,256]{1,0:T(8,128)(2,1)} %refs_0_.1, bf16[768,256]{1,0:T(8,128)(2,1)} %refs_1_.1, bf16[768,256]{1,0:T(8,128)(2,1)} %refs_2_.1, bf16[128,1024]{1,0:T(8,128)(2,1)} %refs_3_.1, ...), custom_call_target="tpu_custom_call" | custom-call | tf_op jit(solution)/shard_map/pallas_call | solution.py:495
  102.9 1.8 %copy.17 = bf16[768,256]{1,0:T(8,128)(2,1)} copy(bf16[768,256]{1,0:T(8,128)(2,1)} %get-tuple-element.10) | data formatting | bytes 786432
  104.7 0.0 copy-start.2
  104.7 0.0 copy-start.1
  104.7 2.7 %copy.18 = bf16[768,1024]{1,0:T(8,128)(2,1)} copy(bf16[768,1024]{1,0:T(8,128)(2,1)} %get-tuple-element.11) | data formatting | bytes 3145728
  107.4 0.0 copy-done.2
  107.4 0.0 copy-start
  107.4 0.7 copy.19
  108.2 0.0 copy-done.1
  108.2 0.8 copy.20
  109.0 0.0 copy-done
  109.0 0.8 copy.21
Async XLA Ops:
  104.7 2.8 %copy-start.2 = (bf16[768,256]{1,0:T(8,128)(2,1)S(1)}, bf16[768,256]{1,0:T(8,128)(2,1)}, u32[]{:S(2)}) copy-start(bf16[768,256]{1,0:T(8,128)(2,1)} %get-tuple-element.12) | copy-start | bytes 1179652
  104.7 3.5 %copy-start.1 = (f32[128,1024]{1,0:T(8,128)S(1)}, f32[128,1024]{1,0:T(8,128)}, u32[]{:S(2)}) copy-start(f32[128,1024]{1,0:T(8,128)} %get-tuple-element.13) | copy-start | bytes 1572868
  107.4 1.5 %copy-start = (f32[128,1024]{1,0:T(8,128)S(1)}, f32[128,1024]{1,0:T(8,128)}, u32[]{:S(2)}) copy-start(f32[128,1024]{1,0:T(8,128)} %get-tuple-element.14) | copy-start | bytes 1572868

commit v3 on v2

v3 whole, which is shorter than its diff:
```python
import jax
import jax.numpy as jnp
from jax import lax
from jax.experimental import pallas as pl
from jax.experimental.pallas import tpu as pltpu
from jax.sharding import PartitionSpec as P

contract_last = (((1,), (1,)), ((), ()))
contract_first = (((0,), (0,)), ((), ()))
bf16, f32 = jnp.bfloat16, jnp.float32
MESH = pl.DeviceIdType.MESH
SIDE = 4
ROWS, WIDTH, MODEL, HIDDEN = 768, 256, 2048, 1024
HALF = HIDDEN // 2
STRIP = ROWS // 2
LIMIT = 60 * 2**20


def around(k):
    return lax.rem(k + SIDE, SIDE)


class Place:
    def __init__(self):
        fs, tp = lax.axis_index("fs"), lax.axis_index("tp")
        self.z, self.x = fs // SIDE, lax.rem(fs, SIDE)
        self.y, self.core = tp // 2, lax.rem(tp, 2)

    def device(self, z=0, x=0, y=0, core=0):
        fs = around(self.z + z) * SIDE + around(self.x + x)
        tp = around(self.y + y) * 2 + lax.rem(self.core + core, 2)
        return (fs, tp)

    def neighbours(self):
        return [self.device(**{a: d}) for a in ("z", "x", "y") for d in (1, -1)] + [
            self.device(core=1)
        ]


class Ring:
    def __init__(self, place, axis, piece, two, sems, base):
        self.sems, self.base, self.two = sems, base, two
        at = getattr(place, axis)
        on, back = place.device(**{axis: 1}), place.device(**{axis: -1})
        before, after, across = around(at - 1), around(at + 1), around(at + 2)
        self.sent = [
            (piece(at, 0), on),
            (piece(at, 1), on),
            (piece(at, 1), back),
            (piece(at, 0), back),
            (piece(before, 0), on),
            (piece(after, 1), back),
        ]

    def copy(self, j, ref):
        send, receive = self.sems
        return pltpu.make_async_remote_copy(
            src_ref=ref,
            dst_ref=ref,
            send_sem=send,
            recv_sem=receive.at[self.base + (0, 1, 0, 1, 2, 2)[j]],
            device_id=self.sent[j][1],
            device_id_type=MESH,
        )

    def start(self, *which):
        for j in which:
            self.copy(j, self.sent[j][0]).start()

    def arrive(self, j):
        self.copy(j, self.two).wait_recv()

    def own(self):
        self.start(0, 2, 1, 3)

    def forward(self):
        self.arrive(0)
        self.start(4, 5)

    def near(self):
        self.arrive(1)

    def far(self):
        self.arrive(4)


class Partner:
    def __init__(self, place, block, three, sems, base):
        self.sems, self.base, self.three = sems, base, three
        self.device = place.device(core=1)
        steps = (0, -1, 1, 2)
        self.sent = [block(around(place.y + d), place.core) for d in steps]

    def copy(self, j, ref):
        send, receive = self.sems
        return pltpu.make_async_remote_copy(
            src_ref=ref,
            dst_ref=ref,
            send_sem=send,
            recv_sem=receive.at[self.base + j // 3],
            device_id=self.device,
            device_id_type=MESH,
        )

    def start(self, *which):
        for j in which:
            self.copy(j, self.sent[j]).start()

    def most(self):
        self.copy(0, self.three).wait_recv()

    def last(self):
        self.copy(3, self.sent[3]).wait_recv()


class RingSum:
    def __init__(self, place, axis, block, far, near, sems, base):
        self.sems, self.base, self.both_near = sems, base, near(slice(None), slice(None))
        at = getattr(place, axis)
        on, back = place.device(**{axis: 1}), place.device(**{axis: -1})
        before, after, across = around(at - 1), around(at + 1), around(at + 2)
        self.mine = [block(at, s) for s in range(2)]
        self.far, self.near = far, near
        self.sent = [
            (block(across, 0), far(0), on),
            (block(across, 1), far(1), back),
            (block(after, 1), near(0, 1), on),
            (block(before, 0), near(1, 0), back),
            (block(after, 0), near(0, 0), on),
            (block(before, 1), near(1, 1), back),
        ]

    def copy(self, j):
        send, receive = self.sems
        src, dst, device = self.sent[j]
        return pltpu.make_async_remote_copy(
            src_ref=src,
            dst_ref=dst,
            send_sem=send,
            recv_sem=receive.at[self.base + (0, 1, 2, 2, 2, 2)[j]],
            device_id=device,
            device_id_type=MESH,
        )

    def start(self, *which):
        for j in which:
            self.copy(j).start()

    def begin(self):
        self.start(0, 1, 2, 3)

    def middle(self):
        for j in range(2):
            self.copy(j).wait_recv()
            ref = self.sent[4 + j][0]
            ref[...] = (ref[...].astype(f32) + self.far(j)[...].astype(f32)).astype(bf16)
            self.copy(4 + j).start()

    def total(self, s):
        return (
            self.mine[s][...].astype(f32)
            + self.near(0, s)[...].astype(f32)
            + self.near(1, s)[...].astype(f32)
        )

    def arrive(self):
        send, receive = self.sems
        pltpu.make_async_remote_copy(
            src_ref=self.both_near,
            dst_ref=self.both_near,
            send_sem=send,
            recv_sem=receive.at[self.base + 2],
            device_id=self.sent[0][2],
            device_id_type=MESH,
        ).wait_recv()

    def finish(self, result=None):
        self.arrive()
        for s in range(2):
            target = self.mine[s] if result is None else result.at[pl.ds(s * STRIP, STRIP), :]
            target[...] = self.total(s).astype(bf16)


def dot(a, b):
    return jnp.dot(a, b, preferred_element_type=f32)


def dot_turned(a, b):
    return lax.dot_general(a, b, contract_last, preferred_element_type=f32)


def layer_kernel(
    factor,
    later_in, earlier_in, cot_in, up_in, down_in, up_run_in, down_run_in,
    later_out_ref, pre, back_out, up_run, down_run,
    act, turned, up, down, first_up, hidden, early_hidden, grad, part, other, up_sum, down_sum,
    far_row, near_row, far_one, near_one, far_two, near_two,
    load_sem, send_sem, ring_recv, pair_recv, sum_recv,
):
    place = Place()
    barrier = pltpu.get_barrier_semaphore()
    for neighbour in place.neighbours():
        pl.semaphore_signal(barrier, inc=1, device_id=neighbour, device_id_type=MESH)

    def act_at(a, y, core, first, count):
        column = pl.multiple_of((y * 2 + core) * WIDTH, WIDTH)
        return act.at[a, pl.ds(first, count), pl.ds(column, WIDTH)]

    def down_at(h, s, first, count):
        return down.at[pl.ds(h * HALF + s * 256, 256), pl.ds(pl.multiple_of(first * 128, 128), count)]

    here = place.z * SIDE + place.x
    loads = [(up_in.at[:, pl.ds(h * HALF, HALF)], up.at[h, place.z, place.x]) for h in range(2)]
    loads.insert(1, (down_in, down.at[:, pl.ds(pl.multiple_of(here * 128, 128), 128)]))
    for a, ref in enumerate((earlier_in, cot_in, later_in)):
        loads.insert(2 + 2 * a, (ref, act_at(a, place.y, place.core, 0, ROWS)))
    loads += [(up_run_in, up_run), (down_run_in, down_run)]
    loads = [pltpu.make_async_copy(s, d, load_sem.at[i]) for i, (s, d) in enumerate(loads)]
    for load in loads:
        load.start()

    sems, block = (send_sem.at[0], ring_recv), up.at[0, 0, 0]
    rings = iter(range(0, 69, 3))
    rows = [
        Ring(place, "y", lambda k, s, a=a: act_at(a, k, place.core, s * 384, 384), act.at[a, :, pl.ds(0, WIDTH)],
            (send_sem.at[6], ring_recv), next(rings))
        for a in range(3)
    ]
    pairs = [
        Partner(place, lambda y, c, a=a: act_at(a, y, c, 0, ROWS), act.at[a, :, pl.ds(0, 3 * WIDTH)], (send_sem.at[1], pair_recv), 2 * a)
        for a in range(3)
    ]
    first, second = [], []
    for h in range(2):
        first.append((
            Ring(place, "z", lambda k, s, h=h: up.at[h, k, place.x, pl.ds(s * 64, 64), :], block, sems, next(rings)),
            Ring(place, "x", lambda k, s, h=h: down_at(h, s, place.z * SIDE + k, 128), block, sems, next(rings)),
        ))
        second.append([])
        for d in (0, -1, 1, 2):
            z, x = around(place.z + d), around(place.x + d)
            second[h].append((
                Ring(place, "x", lambda k, s, h=h, z=z: up.at[h, z, k, pl.ds(s * 64, 64), :], block, sems, next(rings)),
                Ring(place, "z", lambda k, s, h=h, x=x: down_at(h, s, k * SIDE + x, 128), block, sems, next(rings)),
            ))

    sums = iter(range(0, 30, 3))
    row_sums = [
        RingSum(
            place, "y", lambda k, s, a=a: part.at[a, place.core, k, pl.ds(s * 384, 384), :],
            lambda d, a=a: far_row.at[a, d], lambda d, s, a=a: near_row.at[a, d, s], (send_sem.at[2], sum_recv), next(sums),
        )
        for a in range(2)
    ]
    up_one, up_two, down_one, down_two = [], [], [], []
    for h in range(2):
        up_one.append(RingSum(
            place, "x", lambda k, s, h=h: up_sum.at[h, :, k, pl.ds(s * 64, 64), :],
            lambda d, h=h: far_one.at[0, h, d], lambda d, s, h=h: near_one.at[0, h, d, s], (send_sem.at[3], sum_recv), next(sums),
        ))
        down_one.append(RingSum(
            place, "z", lambda k, s, h=h: down_sum.at[h, k, :, pl.ds(s * 64, 64), :],
            lambda d, h=h: far_one.at[1, h, d], lambda d, s, h=h: near_one.at[1, h, d, s], (send_sem.at[3], sum_recv), next(sums),
        ))
        up_two.append(RingSum(
            place, "z", lambda k, s, h=h: up_sum.at[h, k, place.x, pl.ds(s * 64, 64), :],
            lambda d, h=h: far_two.at[0, h, d], lambda d, s, h=h: near_two.at[0, h, d, s], (send_sem.at[4], sum_recv), next(sums),
        ))
        down_two.append(RingSum(
            place, "x", lambda k, s, h=h: down_sum.at[h, place.z, k, pl.ds(s * 64, 64), :],
            lambda d, h=h: far_two.at[1, h, d], lambda d, s, h=h: near_two.at[1, h, d, s], (send_sem.at[4], sum_recv), next(sums),
        ))

    order = [around(place.y + d) for d in (2, 1, -1, 0)]

    def swap(a, i):
        return pltpu.make_async_remote_copy(
            src_ref=part.at[a, 1 - place.core, order[i]],
            dst_ref=other.at[a, order[i]],
            send_sem=send_sem.at[5],
            recv_sem=pair_recv.at[6 + 4 * a + i],
            device_id=place.device(core=1),
            device_id_type=MESH,
        )

    def sent(i, ref):
        pltpu.make_async_remote_copy(
            src_ref=ref,
            dst_ref=ref,
            send_sem=send_sem.at[i],
            recv_sem=pair_recv.at[0],
            device_id=place.device(core=1),
            device_id_type=MESH,
        ).wait_send()

    def both(stage, name):
        for ring in stage:
            getattr(ring, name)()

    def strip(m):
        return pl.ds(pl.multiple_of(m * STRIP, STRIP), STRIP)

    def columns(h):
        return pl.ds(h * HALF, HALF)

    def turn(a, core, start, stop):
        @pl.loop(start, stop)
        def _(d):
            block = pl.ds(pl.multiple_of((around(place.y + d) * 2 + core) * WIDTH, WIDTH), WIDTH)
            turned[a, block, :] = act[a, :, block].T

    def up_of(h):
        return up[h].reshape(MODEL, HALF)

    def earlier_up(h):
        @pl.loop(0, 2)
        def _(m):
            value = jnp.maximum(dot(act[0, strip(m), :], up_of(h)), 0.0)
            first_up[strip(m), :] = value
            early_hidden[strip(m), columns(h)] = jnp.square(value).astype(bf16)

    def hidden_grad(h):
        @pl.loop(0, 2)
        def _(m):
            value = dot_turned(act[1, strip(m), :], down[columns(h), :])
            grad[strip(m), columns(h)] = (2.0 * first_up[strip(m), :] * value).astype(bf16)

    def weight_grad(a, source, target, h):
        @pl.loop(0, 4)
        def _(n):
            block = pl.ds(pl.multiple_of(n * 512, 512), 512)
            value = dot(turned[a, block, :], source[:, columns(h)])
            target[h, n] = value.astype(bf16).reshape(SIDE, 128, HALF)

    def later_up(h):
        @pl.loop(0, 2)
        def _(m):
            value = dot(act[2, strip(m), :], up_of(h))
            pre[strip(m), columns(h)] = value.astype(bf16)
            hidden[strip(m), columns(h)] = jnp.square(jnp.maximum(value, 0.0)).astype(bf16)

    def keep(a, n, m, value):
        value = value.astype(bf16)
        part[a, 0, n, strip(m), :] = value[:, :WIDTH]
        part[a, 1, n, strip(m), :] = value[:, WIDTH:]

    def later_out(i):
        n = order[i]
        block = pl.ds(pl.multiple_of(n * 512, 512), 512)

        @pl.loop(0, 2)
        def _(m):
            keep(0, n, m, dot(hidden[strip(m), :], down[:, block]))

        swap(0, i).start()

    def input_grad(i):
        n = order[i]

        @pl.loop(0, 2)
        def _(m):
            weight = jnp.concatenate([up[h, n].reshape(512, HALF) for h in range(2)], axis=1)
            keep(1, n, m, dot_turned(grad[strip(m), :], weight))

        swap(1, i).start()

    def join(a, i):
        swap(a, i).wait_recv()
        n = order[i]
        part[a, place.core, n] = (
            part[a, place.core, n].astype(f32) + other[a, n].astype(f32)
        ).astype(bf16)
        row_sums[a].start(*((0, 1), (2,), (3,), ())[i])

    def add_running(w, ring, h):
        ring.arrive()
        for s in range(2):
            at = (up_run, down_run)[w].at[pl.ds(s * 64, 64), columns(h)]
            at[...] = at[...] + ring.total(s) * factor

    pl.semaphore_wait(barrier, 7)
    loads[0].wait()
    loads[1].wait()

    both(first[0], "own")
    both(second[0][0], "own")
    loads[2].wait()
    rows[0].own()
    pairs[0].start(0)
    for load in loads[3:]:
        load.wait()
    both(first[0], "forward")
    both(first[0], "near")
    both(second[0][1], "own")
    both(second[0][2], "own")
    both(second[0][0], "forward")
    rows[0].forward()
    rows[1].own()
    pairs[1].start(0)
    both(first[0], "far")
    both(second[0][3], "own")
    both(second[0][1], "forward")
    rows[0].near()
    pairs[0].start(1, 2)
    both(second[0][2], "forward")
    rows[0].far()
    pairs[0].start(3)
    both(second[0][3], "forward")
    both(first[1], "own")
    both(second[1][0], "own")
    pairs[0].most()
    pairs[0].last()
    rows[1].forward()
    rows[2].own()
    pairs[2].start(0)
    turn(0, place.core, -1, 3)
    turn(0, 1 - place.core, -1, 3)
    rows[1].near()
    pairs[1].start(1, 2)
    for ring in second[0]:
        both(ring, "near")
        both(ring, "far")
    both(first[1], "forward")
    both(first[1], "near")
    both(second[1][1], "own")
    both(second[1][2], "own")
    earlier_up(0)
    rows[1].far()
    pairs[1].start(3)
    both(second[1][0], "forward")
    turn(1, place.core, -1, 3)
    pairs[1].most()
    turn(1, 1 - place.core, -1, 2)
    both(first[1], "far")
    both(second[1][3], "own")
    pairs[1].last()
    turn(1, 1 - place.core, 2, 3)
    hidden_grad(0)
    rows[2].forward()
    both(second[1][1], "forward")
    weight_grad(1, early_hidden, down_sum, 0)
    both(second[1][2], "forward")
    rows[2].near()
    pairs[2].start(1, 2)
    weight_grad(0, grad, up_sum, 0)
    both(second[1][3], "forward")
    down_one[0].begin()
    up_one[0].begin()
    rows[2].far()
    pairs[2].start(3)
    pairs[2].most()
    pairs[2].last()
    later_up(0)
    for ring in second[1]:
        both(ring, "near")
        both(ring, "far")
    earlier_up(1)
    hidden_grad(1)
    input_grad(0)
    input_grad(1)
    input_grad(2)
    join(1, 0)
    down_one[0].middle()
    up_one[0].middle()
    input_grad(3)
    join(1, 1)
    weight_grad(1, early_hidden, down_sum, 1)
    down_one[1].begin()
    join(1, 2)
    weight_grad(0, grad, up_sum, 1)
    up_one[1].begin()
    join(1, 3)
    later_up(1)
    row_sums[1].middle()
    later_out(0)
    later_out(1)
    down_one[0].finish()
    up_one[0].finish()
    later_out(2)
    join(0, 0)
    later_out(3)
    join(0, 1)
    down_one[1].middle()
    up_one[1].middle()
    down_two[0].begin()
    up_two[0].begin()
    join(0, 2)
    join(0, 3)
    row_sums[1].finish(back_out)
    row_sums[0].middle()
    down_one[1].finish()
    down_two[1].begin()
    up_one[1].finish()
    up_two[1].begin()
    down_two[0].middle()
    up_two[0].middle()
    row_sums[0].finish(later_out_ref)
    down_two[1].middle()
    up_two[1].middle()
    add_running(1, down_two[0], 0)
    add_running(0, up_two[0], 0)
    add_running(1, down_two[1], 1)
    add_running(0, up_two[1], 1)
    sent(0, act.at[:, pl.ds(0, 640), :])
    sent(1, act.at[:, pl.ds(0, 384), :])
    sent(2, act.at[0, pl.ds(0, 576), :])
    sent(3, act.at[pl.ds(0, 2)])
    sent(4, act.at[0, pl.ds(0, 384), :])
    sent(5, act.at[0])
    sent(6, act.at[pl.ds(0, 2), pl.ds(0, 432), :])


def store_kernel(*refs):
    sources, results, sem = refs[:5], refs[5:10], refs[10]
    copies = [
        pltpu.make_async_copy(src, dst, sem.at[i]) for i, (src, dst) in enumerate(zip(sources, results))
    ]
    for copy in copies:
        copy.start()
    for copy in copies:
        copy.wait()


def on_device(*arrays):
    factor = float(ROWS * 16) ** (-0.5)
    anywhere = pl.BlockSpec(memory_space=pl.ANY)
    inside = pl.BlockSpec(memory_space=pltpu.VMEM)
    kept = [
        ((ROWS, WIDTH), bf16),
        ((ROWS, HIDDEN), bf16),
        ((ROWS, WIDTH), bf16),
        ((128, HIDDEN), f32),
        ((128, HIDDEN), f32),
    ]
    results = pl.pallas_call(
        lambda *refs: layer_kernel(factor, *refs),
        out_shape=tuple(pltpu.VMEM(shape, kind) for shape, kind in kept),
        in_specs=[anywhere] * 7,
        out_specs=(inside,) * 5,
        scratch_shapes=[
            pltpu.VMEM((3, ROWS, MODEL), bf16),
            pltpu.VMEM((2, MODEL, ROWS), bf16),
            pltpu.VMEM((2, SIDE, SIDE, 128, HALF), bf16),
            pltpu.VMEM((HIDDEN, MODEL), bf16),
            pltpu.VMEM((ROWS, HALF), f32),
            pltpu.VMEM((ROWS, HIDDEN), bf16),
            pltpu.VMEM((ROWS, HIDDEN), bf16),
            pltpu.VMEM((ROWS, HIDDEN), bf16),
            pltpu.VMEM((2, 2, SIDE, ROWS, WIDTH), bf16),
            pltpu.VMEM((2, SIDE, ROWS, WIDTH), bf16),
            pltpu.VMEM((2, SIDE, SIDE, 128, HALF), bf16),
            pltpu.VMEM((2, SIDE, SIDE, 128, HALF), bf16),
            pltpu.VMEM((2, 2, STRIP, WIDTH), bf16),
            pltpu.VMEM((2, 2, 2, STRIP, WIDTH), bf16),
            pltpu.VMEM((2, 2, 2, SIDE, 64, HALF), bf16),
            pltpu.VMEM((2, 2, 2, 2, SIDE, 64, HALF), bf16),
            pltpu.VMEM((2, 2, 2, 64, HALF), bf16),
            pltpu.VMEM((2, 2, 2, 2, 64, HALF), bf16),
            pltpu.SemaphoreType.DMA((8,)),
            pltpu.SemaphoreType.DMA((7,)),
            pltpu.SemaphoreType.DMA((69,)),
            pltpu.SemaphoreType.DMA((14,)),
            pltpu.SemaphoreType.DMA((30,)),
        ],
        compiler_params=pltpu.CompilerParams(
            collective_id=0, has_side_effects=True, vmem_limit_bytes=LIMIT
        ),
    )(*arrays)
    return pl.pallas_call(
        store_kernel,
        out_shape=tuple(jax.ShapeDtypeStruct(shape, kind) for shape, kind in kept),
        in_specs=[inside] * 5,
        out_specs=(anywhere,) * 5,
        scratch_shapes=[pltpu.SemaphoreType.DMA((5,))],
        compiler_params=pltpu.CompilerParams(vmem_limit_bytes=2**20),
    )(*[pltpu.with_memory_space_constraint(r, pltpu.VMEM) for r in results])


def solution(mesh):
    in_specs = (
        P("fs", "tp"),
        P("fs", "tp"),
        P("fs", "tp"),
        P("fs", "tp"),
        P("tp", "fs"),
        P("fs", "tp"),
        P("fs", "tp"),
    )
    out_specs = (P("fs", "tp"),) * 5
    return jax.shard_map(
        on_device, mesh=mesh, in_specs=in_specs, out_specs=out_specs, check_vma=False
    )
```

time: 111 us -> 98 us (0.88); the launches traced: 110 us -> 97.9 us
  local copies, waits for them, and re-layouts: 6.86 us -> 0 us
  Pallas kernels: 102 us -> 97.3 us
    unnamed x11 -> x0, local copies, waits for them, and re-layouts: 6.86 us -> none
    pallas_call x1 -> x2, Pallas kernels: 102 us -> 97.3 us  [the longest x1 95.5 us: on_device(): pl.pallas_call(lambda *refs: layer_kernel(factor, *refs), out_shape=tuple...]
where the time goes in v3:
time: 98 us; the launch traced here: 97.9 us
  Pallas kernels  97.3 us (99%)
    pallas_call x1, Pallas kernels, on_device(): pl.pallas_call(lambda *refs: layer_kernel(factor, *refs), out_shape=tuple...  95.5 us

profile of v3, /device:TPU:0, one launch (start us, length us, event | category | flops | bytes accessed | tf_op | source)
XLA Modules:
  0.0 97.9 jit_solution(340616298077383115)
XLA Ops:
  0.6 95.5 %shard_map.110 = (bf16[768,256]{1,0:T(8,128)(2,1)S(1)}, bf16[768,1024]{1,0:T(8,128)(2,1)S(1)}, bf16[768,256]{1,0:T(8,128)(2,1)S(1)}, f32[128,1024]{1,0:T(8,128)S(1)}, f32[128,1024]{1,0:T(8,128)S(1)}) custom-call(bf16[768,256]{1,0:T(8,128)(2,1)} %refs_0_.1, bf16[768,256]{1,0:T(8,128)(2,1)} %refs_1_.1, bf16[768,256]{1,0:T(8,128)(2,1)} %refs_2_.1, ...), custom_call_target="tpu_custom_call" | custom-call | tf_op jit(solution)/shard_map/pallas_call | solution.py:535
  96.1 1.8 %shard_map.111 = (bf16[768,256]{1,0:T(8,128)(2,1)}, bf16[768,1024]{1,0:T(8,128)(2,1)}, bf16[768,256]{1,0:T(8,128)(2,1)}, f32[128,1024]{1,0:T(8,128)}, f32[128,1024]{1,0:T(8,128)}) custom-call(bf16[768,256]{1,0:T(8,128)(2,1)S(1)} %get-tuple-element.10.refs_0_, bf16[768,1024]{1,0:T(8,128)(2,1)S(1)} %get-tuple-element.11.refs_1_, ...), custom_call_target="tpu_custom_call" | custom-call | tf_op jit(solution)/shard_map/pallas_call | solution.py:569

commit v4 on v3

--- a/solution.py
+++ b/solution.py
@@ -38,8 +38,11 @@
 
 
 class Ring:
-    def __init__(self, place, axis, piece, two, sems, base):
-        self.sems, self.base, self.two = sems, base, two
+    def __init__(self, place, axis, piece, two, sems, bases, four=None):
+        self.sems, self.two, self.four = sems, two, four
+        self.last = 2 if four is None else 1
+        self.base = bases[0]
+        del bases[: self.last + 1]
         at = getattr(place, axis)
         on, back = place.device(**{axis: 1}), place.device(**{axis: -1})
         before, after, across = around(at - 1), around(at + 1), around(at + 2)
@@ -58,7 +61,7 @@
             src_ref=ref,
             dst_ref=ref,
             send_sem=send,
-            recv_sem=receive.at[self.base + (0, 1, 0, 1, 2, 2)[j]],
+            recv_sem=receive.at[self.base + (0, 1, 0, 1, self.last, self.last)[j]],
             device_id=self.sent[j][1],
             device_id_type=MESH,
         )
@@ -82,6 +85,9 @@
 
     def far(self):
         self.arrive(4)
+
+    def rest(self):
+        self.copy(1, self.four).wait_recv()
 
 
 class Partner:
@@ -115,7 +121,8 @@
 
 class RingSum:
     def __init__(self, place, axis, block, far, near, sems, base):
-        self.sems, self.base, self.both_near = sems, base, near(slice(None), slice(None))
+        self.sems, self.base = sems, base
+        self.both_far, self.both_near = far(slice(None)), near(slice(None), slice(None))
         at = getattr(place, axis)
         on, back = place.device(**{axis: 1}), place.device(**{axis: -1})
         before, after, across = around(at - 1), around(at + 1), around(at + 2)
@@ -137,7 +144,7 @@
             src_ref=src,
             dst_ref=dst,
             send_sem=send,
-            recv_sem=receive.at[self.base + (0, 1, 2, 2, 2, 2)[j]],
+            recv_sem=receive.at[self.base + (0, 0, 1, 1, 1, 1)[j]],
             device_id=device,
             device_id_type=MESH,
         )
@@ -149,12 +156,23 @@
     def begin(self):
         self.start(0, 1, 2, 3)
 
+    def receive(self, ref, k):
+        send, receive = self.sems
+        pltpu.make_async_remote_copy(
+            src_ref=ref,
+            dst_ref=ref,
+            send_sem=send,
+            recv_sem=receive.at[self.base + k],
+            device_id=self.sent[0][2],
+            device_id_type=MESH,
+        ).wait_recv()
+
     def middle(self):
+        self.receive(self.both_far, 0)
         for j in range(2):
-            self.copy(j).wait_recv()
             ref = self.sent[4 + j][0]
             ref[...] = (ref[...].astype(f32) + self.far(j)[...].astype(f32)).astype(bf16)
-            self.copy(4 + j).start()
+        self.start(4, 5)
 
     def total(self, s):
         return (
@@ -164,15 +182,7 @@
         )
 
     def arrive(self):
-        send, receive = self.sems
-        pltpu.make_async_remote_copy(
-            src_ref=self.both_near,
-            dst_ref=self.both_near,
-            send_sem=send,
-            recv_sem=receive.at[self.base + 2],
-            device_id=self.sent[0][2],
-            device_id_type=MESH,
-        ).wait_recv()
+        self.receive(self.both_near, 1)
 
     def finish(self, result=None):
         self.arrive()
@@ -219,11 +229,11 @@
     for load in loads:
         load.start()
 
-    sems, block = (send_sem.at[0], ring_recv), up.at[0, 0, 0]
-    rings = iter(range(0, 69, 3))
+    sems, block, pair = (send_sem.at[0], ring_recv), up.at[0, 0, 0], up.at[0, 0, pl.ds(0, 2)]
+    rings = list(range(41))
     rows = [
         Ring(place, "y", lambda k, s, a=a: act_at(a, k, place.core, s * 384, 384), act.at[a, :, pl.ds(0, WIDTH)],
-            (send_sem.at[6], ring_recv), next(rings))
+            (send_sem.at[6], ring_recv), rings)
         for a in range(3)
     ]
     pairs = [
@@ -233,18 +243,21 @@
     first, second = [], []
     for h in range(2):
         first.append((
-            Ring(place, "z", lambda k, s, h=h: up.at[h, k, place.x, pl.ds(s * 64, 64), :], block, sems, next(rings)),
-            Ring(place, "x", lambda k, s, h=h: down_at(h, s, place.z * SIDE + k, 128), block, sems, next(rings)),
+            Ring(place, "z", lambda k, s, h=h: up.at[h, k, place.x, pl.ds(s * 64, 64), :], block, sems, rings),
+            Ring(place, "x", lambda k, s, h=h: down_at(h, s, place.z * SIDE + k, 128), block, sems, rings),
         ))
-        second.append([])
-        for d in (0, -1, 1, 2):
-            z, x = around(place.z + d), around(place.x + d)
-            second[h].append((
-                Ring(place, "x", lambda k, s, h=h, z=z: up.at[h, z, k, pl.ds(s * 64, 64), :], block, sems, next(rings)),
-                Ring(place, "z", lambda k, s, h=h, x=x: down_at(h, s, k * SIDE + x, 128), block, sems, next(rings)),
-            ))
-
-    sums = iter(range(0, 30, 3))
+    for d in (0, -1, 1, 2):
+        z, x = around(place.z + d), around(place.x + d)
+        second.append((
+            Ring(place, "x", lambda k, s, z=z: up.at[0, z, k, pl.ds(s * 64, 64), :], block, sems, rings, pair),
+            Ring(place, "z", lambda k, s, x=x: down_at(0, s, k * SIDE + x, 128), block, sems, rings, pair),
+        ))
+    last = (
+        Ring(place, "x", lambda k, s: up.at[1, :, k, pl.ds(s * 64, 64), :], up.at[0, 0], sems, rings, up.at[0, pl.ds(0, 2)]),
+        Ring(place, "z", lambda k, s: down_at(1, s, k * SIDE, 512), up.at[0, 0], sems, rings, up.at[0, pl.ds(0, 2)]),
+    )
+
+    sums = iter(range(0, 32, 2))
     row_sums = [
         RingSum(
             place, "y", lambda k, s, a=a: part.at[a, place.core, k, pl.ds(s * 384, 384), :],
@@ -252,23 +265,39 @@
         )
         for a in range(2)
     ]
-    up_one, up_two, down_one, down_two = [], [], [], []
+    one, two = (send_sem.at[3], sum_recv), (send_sem.at[4], sum_recv)
+    first_sums = (
+        RingSum(
+            place, "z", lambda k, s: down_sum.at[0, k, :, pl.ds(s * 64, 64), :],
+            lambda d: far_one.at[1, 0, d], lambda d, s: near_one.at[1, 0, d, s], one, next(sums),
+        ),
+        RingSum(
+            place, "x", lambda k, s: up_sum.at[0, :, k, pl.ds(s * 64, 64), :],
+            lambda d: far_one.at[0, 0, d], lambda d, s: near_one.at[0, 0, d, s], one, next(sums),
+        ),
+    )
+    down_lines, up_lines, second_sums = [], [], []
+    for q in (2, 1, -1, 0):
+        z, x = around(place.z + q), around(place.x + q)
+        down_lines.append(RingSum(
+            place, "z", lambda k, s, x=x: down_sum.at[1, k, x, pl.ds(s * 64, 64), :],
+            lambda d, x=x: far_one.at[1, 1, d, x], lambda d, s, x=x: near_one.at[1, 1, d, s, x], one, next(sums),
+        ))
+        up_lines.append(RingSum(
+            place, "x", lambda k, s, z=z: up_sum.at[1, z, k, pl.ds(s * 64, 64), :],
+            lambda d, z=z: far_one.at[0, 1, d, z], lambda d, s, z=z: near_one.at[0, 1, d, s, z], one, next(sums),
+        ))
+    lines = list(zip(down_lines, up_lines))
     for h in range(2):
-        up_one.append(RingSum(
-            place, "x", lambda k, s, h=h: up_sum.at[h, :, k, pl.ds(s * 64, 64), :],
-            lambda d, h=h: far_one.at[0, h, d], lambda d, s, h=h: near_one.at[0, h, d, s], (send_sem.at[3], sum_recv), next(sums),
-        ))
-        down_one.append(RingSum(
-            place, "z", lambda k, s, h=h: down_sum.at[h, k, :, pl.ds(s * 64, 64), :],
-            lambda d, h=h: far_one.at[1, h, d], lambda d, s, h=h: near_one.at[1, h, d, s], (send_sem.at[3], sum_recv), next(sums),
-        ))
-        up_two.append(RingSum(
-            place, "z", lambda k, s, h=h: up_sum.at[h, k, place.x, pl.ds(s * 64, 64), :],
-            lambda d, h=h: far_two.at[0, h, d], lambda d, s, h=h: near_two.at[0, h, d, s], (send_sem.at[4], sum_recv), next(sums),
-        ))
-        down_two.append(RingSum(
-            place, "x", lambda k, s, h=h: down_sum.at[h, place.z, k, pl.ds(s * 64, 64), :],
-            lambda d, h=h: far_two.at[1, h, d], lambda d, s, h=h: near_two.at[1, h, d, s], (send_sem.at[4], sum_recv), next(sums),
+        second_sums.append((
+            RingSum(
+                place, "x", lambda k, s, h=h: down_sum.at[h, place.z, k, pl.ds(s * 64, 64), :],
+                lambda d, h=h: far_two.at[1, h, d], lambda d, s, h=h: near_two.at[1, h, d, s], two, next(sums),
+            ),
+            RingSum(
+                place, "z", lambda k, s, h=h: up_sum.at[h, k, place.x, pl.ds(s * 64, 64), :],
+                lambda d, h=h: far_two.at[0, h, d], lambda d, s, h=h: near_two.at[0, h, d, s], two, next(sums),
+            ),
         ))
 
     order = [around(place.y + d) for d in (2, 1, -1, 0)]
@@ -383,124 +412,116 @@
     loads[1].wait()
 
     both(first[0], "own")
-    both(second[0][0], "own")
+    both(second[0], "own")
     loads[2].wait()
     rows[0].own()
     pairs[0].start(0)
     for load in loads[3:]:
         load.wait()
     both(first[0], "forward")
+    both(first[1], "own")
     both(first[0], "near")
-    both(second[0][1], "own")
-    both(second[0][2], "own")
-    both(second[0][0], "forward")
+    both(second[1], "own")
+    both(second[2], "own")
+    both(second[0], "forward")
     rows[0].forward()
     rows[1].own()
     pairs[1].start(0)
     both(first[0], "far")
-    both(second[0][3], "own")
-    both(second[0][1], "forward")
+    both(second[3], "own")
+    both(first[1], "forward")
+    both(second[1], "forward")
     rows[0].near()
     pairs[0].start(1, 2)
-    both(second[0][2], "forward")
     rows[0].far()
     pairs[0].start(3)
-    both(second[0][3], "forward")
-    both(first[1], "own")
-    both(second[1][0], "own")
-    pairs[0].most()
-    pairs[0].last()
+    both(second[2], "forward")
+    both(second[3], "forward")
     rows[1].forward()
     rows[2].own()
     pairs[2].start(0)
+    both(first[1], "near")
+    both(first[1], "far")
+    both(last, "own")
+    pairs[0].most()
+    pairs[0].last()
     turn(0, place.core, -1, 3)
     turn(0, 1 - place.core, -1, 3)
     rows[1].near()
     pairs[1].start(1, 2)
-    for ring in second[0]:
-        both(ring, "near")
-        both(ring, "far")
-    both(first[1], "forward")
-    both(first[1], "near")
-    both(second[1][1], "own")
-    both(second[1][2], "own")
+    for ring in second:
+        both(ring, "rest")
     earlier_up(0)
     rows[1].far()
     pairs[1].start(3)
-    both(second[1][0], "forward")
     turn(1, place.core, -1, 3)
     pairs[1].most()
     turn(1, 1 - place.core, -1, 2)
-    both(first[1], "far")
-    both(second[1][3], "own")
     pairs[1].last()
     turn(1, 1 - place.core, 2, 3)
+    rows[2].forward()
+    both(last, "forward")
+    weight_grad(1, early_hidden, down_sum, 0)
+    first_sums[0].begin()
     hidden_grad(0)
-    rows[2].forward()
-    both(second[1][1], "forward")
-    weight_grad(1, early_hidden, down_sum, 0)
-    both(second[1][2], "forward")
     rows[2].near()
     pairs[2].start(1, 2)
     weight_grad(0, grad, up_sum, 0)
-    both(second[1][3], "forward")
-    down_one[0].begin()
-    up_one[0].begin()
+    first_sums[1].begin()
     rows[2].far()
     pairs[2].start(3)
     pairs[2].most()
     pairs[2].last()
     later_up(0)
-    for ring in second[1]:
-        both(ring, "near")
-        both(ring, "far")
+    both(last, "rest")
     earlier_up(1)
     hidden_grad(1)
     input_grad(0)
     input_grad(1)
+    both(first_sums, "middle")
+    weight_grad(1, early_hidden, down_sum, 1)
+    both(down_lines[:3], "begin")
+    join(1, 0)
+    weight_grad(0, grad, up_sum, 1)
+    both(up_lines[:3], "begin")
+    join(1, 1)
     input_grad(2)
-    join(1, 0)
-    down_one[0].middle()
-    up_one[0].middle()
     input_grad(3)
-    join(1, 1)
-    weight_grad(1, early_hidden, down_sum, 1)
-    down_one[1].begin()
+    later_up(1)
     join(1, 2)
-    weight_grad(0, grad, up_sum, 1)
-    up_one[1].begin()
     join(1, 3)
-    later_up(1)
+    both(first_sums, "finish")
+    both(second_sums[0], "begin")
     row_sums[1].middle()
     later_out(0)
     later_out(1)
-    down_one[0].finish()
-    up_one[0].finish()
+    for line in lines[:3]:
+        both(line, "middle")
+    both(lines[3], "begin")
     later_out(2)
     join(0, 0)
     later_out(3)
     join(0, 1)
-    down_one[1].middle()
-    up_one[1].middle()
-    down_two[0].begin()
-    up_two[0].begin()
+    both(second_sums[0], "middle")
     join(0, 2)
     join(0, 3)
     row_sums[1].finish(back_out)
     row_sums[0].middle()
-    down_one[1].finish()
-    down_two[1].begin()
-    up_one[1].finish()
-    up_two[1].begin()
-    down_two[0].middle()
-    up_two[0].middle()
+    both(lines[0], "finish")
+    for ring in second_sums[1]:
+        ring.start(0, 1)
+    both(lines[1], "finish")
+    both(lines[2], "finish")
+    for ring in second_sums[1]:
+        ring.start(2, 3)
+    both(lines[3], "middle")
+    both(second_sums[1], "middle")
+    add_running(1, second_sums[0][0], 0)
+    add_running(0, second_sums[0][1], 0)
     row_sums[0].finish(later_out_ref)
-    down_two[1].middle()
-    up_two[1].middle()
-    add_running(1, down_two[0], 0)
-    add_running(0, up_two[0], 0)
-    add_running(1, down_two[1], 1)
-    add_running(0, up_two[1], 1)
+    both(lines[3], "finish")
+    add_running(1, second_sums[1][0], 1)
+    add_running(0, second_sums[1][1], 1)
     sent(0, act.at[:, pl.ds(0, 640), :])
     sent(1, act.at[:, pl.ds(0, 384), :])
     sent(2, act.at[0, pl.ds(0, 576), :])
@@ -558,9 +579,9 @@
             pltpu.VMEM((2, 2, 2, 2, 64, HALF), bf16),
             pltpu.SemaphoreType.DMA((8,)),
             pltpu.SemaphoreType.DMA((7,)),
-            pltpu.SemaphoreType.DMA((69,)),
+            pltpu.SemaphoreType.DMA((41,)),
             pltpu.SemaphoreType.DMA((14,)),
-            pltpu.SemaphoreType.DMA((30,)),
+            pltpu.SemaphoreType.DMA((32,)),
         ],
         compiler_params=pltpu.CompilerParams(
             collective_id=0, has_side_effects=True, vmem_limit_bytes=LIMIT

time: 98 us -> 97.5 us (level)
  no operation moved by 1% of the time
where the time goes in v4:
time: 97.5 us; the launch traced here: 97.4 us
  Pallas kernels  96.8 us (99%)
    pallas_call x1, Pallas kernels, on_device(): pl.pallas_call(lambda *refs: layer_kernel(factor, *refs), out_shape=tuple...  95 us

profile of v4, /device:TPU:0, one launch (start us, length us, event | category | flops | bytes accessed | tf_op | source)
XLA Modules:
  0.0 97.4 jit_solution(10179174185526783817)
XLA Ops:
  0.6 95.0 %shard_map.110 = (bf16[768,256]{1,0:T(8,128)(2,1)S(1)}, bf16[768,1024]{1,0:T(8,128)(2,1)S(1)}, bf16[768,256]{1,0:T(8,128)(2,1)S(1)}, f32[128,1024]{1,0:T(8,128)S(1)}, f32[128,1024]{1,0:T(8,128)S(1)}) custom-call(bf16[768,256]{1,0:T(8,128)(2,1)} %refs_0_.1, bf16[768,256]{1,0:T(8,128)(2,1)} %refs_1_.1, bf16[768,256]{1,0:T(8,128)(2,1)} %refs_2_.1, ...), custom_call_target="tpu_custom_call" | custom-call | tf_op jit(solution)/shard_map/pallas_call | solution.py:556
  95.6 1.8 %shard_map.111 = (bf16[768,256]{1,0:T(8,128)(2,1)}, bf16[768,1024]{1,0:T(8,128)(2,1)}, bf16[768,256]{1,0:T(8,128)(2,1)}, f32[128,1024]{1,0:T(8,128)}, f32[128,1024]{1,0:T(8,128)}) custom-call(bf16[768,256]{1,0:T(8,128)(2,1)S(1)} %get-tuple-element.10.refs_0_, bf16[768,1024]{1,0:T(8,128)(2,1)S(1)} %get-tuple-element.11.refs_1_, ...), custom_call_target="tpu_custom_call" | custom-call | tf_op jit(solution)/shard_map/pallas_call | solution.py:590

commit v5 on v4

--- a/solution.py
+++ b/solution.py
@@ -495,21 +495,21 @@
     row_sums[1].middle()
     later_out(0)
     later_out(1)
-    for line in lines[:3]:
-        both(line, "middle")
-    both(lines[3], "begin")
     later_out(2)
     join(0, 0)
     later_out(3)
     join(0, 1)
+    for line in lines[:3]:
+        both(line, "middle")
+    both(lines[3], "begin")
     both(second_sums[0], "middle")
     join(0, 2)
     join(0, 3)
     row_sums[1].finish(back_out)
-    row_sums[0].middle()
     both(lines[0], "finish")
     for ring in second_sums[1]:
         ring.start(0, 1)
+    row_sums[0].middle()
     both(lines[1], "finish")
     both(lines[2], "finish")
     for ring in second_sums[1]:

time: 97.5 us -> 97.5 us (level)
  no operation moved by 1% of the time
where the time goes in v5:
time: 97.5 us; the launch traced here: 97.4 us
  Pallas kernels  96.8 us (99%)
    pallas_call x1, Pallas kernels, on_device(): pl.pallas_call(lambda *refs: layer_kernel(factor, *refs), out_shape=tuple...  95 us

profile of v5, /device:TPU:0, one launch (start us, length us, event | category | flops | bytes accessed | tf_op | source)
XLA Modules:
  0.0 97.4 jit_solution(4395884798210493968)
XLA Ops:
  0.6 95.0 %shard_map.110 = (bf16[768,256]{1,0:T(8,128)(2,1)S(1)}, bf16[768,1024]{1,0:T(8,128)(2,1)S(1)}, bf16[768,256]{1,0:T(8,128)(2,1)S(1)}, f32[128,1024]{1,0:T(8,128)S(1)}, f32[128,1024]{1,0:T(8,128)S(1)}) custom-call(bf16[768,256]{1,0:T(8,128)(2,1)} %refs_0_.1, bf16[768,256]{1,0:T(8,128)(2,1)} %refs_1_.1, bf16[768,256]{1,0:T(8,128)(2,1)} %refs_2_.1, ...), custom_call_target="tpu_custom_call" | custom-call | tf_op jit(solution)/shard_map/pallas_call | solution.py:556
  95.6 1.8 %shard_map.111 = (bf16[768,256]{1,0:T(8,128)(2,1)}, bf16[768,1024]{1,0:T(8,128)(2,1)}, bf16[768,256]{1,0:T(8,128)(2,1)}, f32[128,1024]{1,0:T(8,128)}, f32[128,1024]{1,0:T(8,128)}) custom-call(bf16[768,256]{1,0:T(8,128)(2,1)S(1)} %get-tuple-element.10.refs_0_, bf16[768,1024]{1,0:T(8,128)(2,1)S(1)} %get-tuple-element.11.refs_1_, ...), custom_call_target="tpu_custom_call" | custom-call | tf_op jit(solution)/shard_map/pallas_call | solution.py:590

commit v6 on v5

v6 whole, which is shorter than its diff:
```python
import jax
import jax.numpy as jnp
from jax import lax
from jax.experimental import pallas as pl
from jax.experimental.pallas import tpu as pltpu
from jax.sharding import PartitionSpec as P

contract_last = (((1,), (1,)), ((), ()))
contract_first = (((0,), (0,)), ((), ()))
bf16, f32 = jnp.bfloat16, jnp.float32
MESH = pl.DeviceIdType.MESH
SIDE = 4
ROWS, WIDTH, MODEL, HIDDEN = 768, 256, 2048, 1024
HALF = HIDDEN // 2
STRIP = ROWS // 2
LIMIT = 60 * 2**20


def around(k):
    return lax.rem(k + SIDE, SIDE)


class Place:
    def __init__(self):
        fs, tp = lax.axis_index("fs"), lax.axis_index("tp")
        self.z, self.x = fs // SIDE, lax.rem(fs, SIDE)
        self.y, self.core = tp // 2, lax.rem(tp, 2)

    def device(self, z=0, x=0, y=0, core=0):
        fs = around(self.z + z) * SIDE + around(self.x + x)
        tp = around(self.y + y) * 2 + lax.rem(self.core + core, 2)
        return (fs, tp)

    def neighbours(self):
        return [self.device(**{a: d}) for a in ("z", "x", "y") for d in (1, -1)] + [
            self.device(core=1)
        ]


def remote(src, dst, device, send, receive):
    return pltpu.make_async_remote_copy(
        src_ref=src, dst_ref=dst, send_sem=send, recv_sem=receive, device_id=device, device_id_type=MESH
    )


class Ring:
    def __init__(self, place, parts, half, bulk, sems, bases, joint=False):
        self.place, self.count, self.bulk, self.sems = place, half * len(parts), bulk, sems
        self.last = 1 if joint else 2
        self.base = bases[0]
        del bases[: self.last + 1]
        self.sent = []
        for axis, piece in parts:
            at = getattr(place, axis)
            on, back = place.device(**{axis: 1}), place.device(**{axis: -1})
            before, after = around(at - 1), around(at + 1)
            self.sent.append([
                (piece(at, 0), on),
                (piece(at, 1), on),
                (piece(at, 1), back),
                (piece(at, 0), back),
                (piece(before, 0), on),
                (piece(after, 1), back),
            ])

    def start(self, *which):
        send, receive = self.sems
        for part in self.sent:
            for j in which:
                ref, device = part[j]
                k = (0, 1, 0, 1, self.last, self.last)[j]
                remote(ref, ref, device, send, receive.at[self.base + k]).start()

    def wait(self, k, halves):
        send, receive = self.sems
        ref = self.bulk(halves * self.count)
        remote(ref, ref, self.place.device(core=1), send, receive.at[self.base + k]).wait_recv()

    def own(self):
        self.start(0, 2, 1, 3)

    def forward(self):
        self.wait(0, 2)
        self.start(4, 5)

    def near(self):
        self.wait(1, 2)

    def far(self):
        self.wait(2, 2)

    def rest(self):
        self.wait(1, 4)


class Partner:
    def __init__(self, place, block, bulk, sems, base, joint):
        self.bulk, self.sems, self.base = bulk, sems, base
        self.keys = (0, 0, 0, 0) if joint else (0, 0, 0, 1)
        self.device = place.device(core=1)
        self.sent = [block(around(place.y + d), place.core) for d in (0, -1, 1, 2)]

    def start(self, *which):
        send, receive = self.sems
        for j in which:
            ref = self.sent[j]
            remote(ref, ref, self.device, send, receive.at[self.base + self.keys[j]]).start()

    def wait(self, k, blocks):
        send, receive = self.sems
        ref = self.bulk(blocks * ROWS * WIDTH)
        remote(ref, ref, self.device, send, receive.at[self.base + k]).wait_recv()


class RingSum:
    def __init__(self, place, parts, half, bulk, sems, base):
        self.place, self.count, self.bulk, self.sems, self.base = place, half * len(parts), bulk, sems, base
        self.mine, self.boxes, self.sent = [], [], []
        for axis, block, far, near in parts:
            at = getattr(place, axis)
            on, back = place.device(**{axis: 1}), place.device(**{axis: -1})
            before, after, across = around(at - 1), around(at + 1), around(at + 2)
            self.mine.append([block(at, s) for s in range(2)])
            self.boxes.append((far, near))
            self.sent.append([
                (block(across, 0), far(0), on),
                (block(across, 1), far(1), back),
                (block(after, 1), near(0, 1), on),
                (block(before, 0), near(1, 0), back),
                (block(after, 0), near(0, 0), on),
                (block(before, 1), near(1, 1), back),
            ])

    def start(self, which, parts=None):
        send, receive = self.sems
        for part in self.sent if parts is None else [self.sent[p] for p in parts]:
            for j in which:
                src, dst, device = part[j]
                remote(src, dst, device, send, receive.at[self.base + (0 if j < 2 else 1)]).start()

    def begin(self, *parts):
        self.start((0, 1, 2, 3), parts or None)

    def wait(self, k, halves):
        send, receive = self.sems
        ref = self.bulk(halves * self.count)
        remote(ref, ref, self.place.device(core=1), send, receive.at[self.base + k]).wait_recv()

    def middle(self):
        self.wait(0, 2)
        for p, (far, near) in enumerate(self.boxes):
            for j in range(2):
                ref = self.sent[p][4 + j][0]
                ref[...] = (ref[...].astype(f32) + far(j)[...].astype(f32)).astype(bf16)
            self.start((4, 5), (p,))

    def arrive(self):
        self.wait(1, 4)

    def total(self, p, s):
        near = self.boxes[p][1]
        return (
            self.mine[p][s][...].astype(f32)
            + near(0, s)[...].astype(f32)
            + near(1, s)[...].astype(f32)
        )

    def finish(self, result=None):
        self.arrive()
        for p, mine in enumerate(self.mine):
            for s in range(2):
                target = mine[s] if result is None else result.at[pl.ds(s * STRIP, STRIP), :]
                target[...] = self.total(p, s).astype(bf16)


def dot(a, b):
    return jnp.dot(a, b, preferred_element_type=f32)


def dot_turned(a, b):
    return lax.dot_general(a, b, contract_last, preferred_element_type=f32)


def layer_kernel(
    factor,
    later_in, earlier_in, cot_in, up_in, down_in, up_run_in, down_run_in,
    later_out_ref, pre, back_out, up_run, down_run,
    act, turned, up, down, first_up, hidden, early_hidden, grad, part, other, up_sum, down_sum,
    far_row, near_row, far_one, near_one, far_two, near_two,
    load_sem, send_sem, ring_recv, pair_recv, sum_recv,
):
    place = Place()
    barrier = pltpu.get_barrier_semaphore()
    for neighbour in place.neighbours():
        pl.semaphore_signal(barrier, inc=1, device_id=neighbour, device_id_type=MESH)

    def act_at(a, y, core, first, count):
        column = pl.multiple_of((y * 2 + core) * WIDTH, WIDTH)
        return act.at[a, pl.ds(first, count), pl.ds(column, WIDTH)]

    def down_at(h, s, first, count):
        return down.at[pl.ds(h * HALF + s * 256, 256), pl.ds(pl.multiple_of(first * 128, 128), count)]

    def bulk(count):
        return act.at[0, pl.ds(0, count // MODEL), :]

    here = place.z * SIDE + place.x
    mine = [act_at(a, place.y, place.core, 0, ROWS) for a in range(3)]
    loads = [
        (up_in.at[:, pl.ds(0, HALF)], up.at[0, place.z, place.x], 0),
        (down_in, down.at[:, pl.ds(pl.multiple_of(here * 128, 128), 128)], 0),
        (earlier_in, mine[0], 1),
        (up_in.at[:, pl.ds(HALF, HALF)], up.at[1, place.z, place.x], 2),
        (cot_in, mine[1], 2),
        (later_in, mine[2], 2),
        (up_run_in, up_run, 2),
        (down_run_in, down_run, 2),
    ]
    for src, dst, k in loads:
        pltpu.make_async_copy(src, dst, load_sem.at[k]).start()

    def loaded(k, count):
        ref = bulk(count)
        pltpu.make_async_copy(ref, ref, load_sem.at[k]).wait()

    bases = list(range(24))
    sems = (send_sem.at[0], ring_recv)
    rows = [
        Ring(
            place, [("y", lambda k, s, a=a: act_at(a, k, place.core, s * STRIP, STRIP))],
            STRIP * WIDTH, bulk, (send_sem.at[2], ring_recv), bases,
        )
        for a in range(3)
    ]
    pairs = [
        Partner(
            place, lambda y, c, a=a: act_at(a, y, c, 0, ROWS), bulk, (send_sem.at[2], pair_recv),
            (0, 1, 3)[a], a != 1,
        )
        for a in range(3)
    ]
    first, second = [], []
    for h in range(2):
        first.append(Ring(
            place,
            [
                ("z", lambda k, s, h=h: up.at[h, k, place.x, pl.ds(s * 64, 64), :]),
                ("x", lambda k, s, h=h: down_at(h, s, place.z * SIDE + k, 128)),
            ],
            64 * HALF, bulk, sems, bases, h == 1,
        ))
    for d in (0, -1, 1, 2):
        z, x = around(place.z + d), around(place.x + d)
        second.append(Ring(
            place,
            [
                ("x", lambda k, s, z=z: up.at[0, z, k, pl.ds(s * 64, 64), :]),
                ("z", lambda k, s, x=x: down_at(0, s, k * SIDE + x, 128)),
            ],
            64 * HALF, bulk, sems, bases, True,
        ))
    last = Ring(
        place,
        [
            ("x", lambda k, s: up.at[1, :, k, pl.ds(s * 64, 64), :]),
            ("z", lambda k, s: down_at(1, s, k * SIDE, 512)),
        ],
        SIDE * 64 * HALF, bulk, sems, bases, True,
    )

    sums = iter(range(0, 18, 2))
    row_sums = [
        RingSum(
            place,
            [(
                "y", lambda k, s, a=a: part.at[a, place.core, k, pl.ds(s * STRIP, STRIP), :],
                lambda d, a=a: far_row.at[a, d], lambda d, s, a=a: near_row.at[a, d, s],
            )],
            STRIP * WIDTH, bulk, (send_sem.at[3], sum_recv), next(sums),
        )
        for a in range(2)
    ]
    sems = (send_sem.at[1], sum_recv)
    first_sum = RingSum(
        place,
        [
            (
                "z", lambda k, s: down_sum.at[0, k, :, pl.ds(s * 64, 64), :],
                lambda d: far_one.at[1, 0, d], lambda d, s: near_one.at[1, 0, d, s],
            ),
            (
                "x", lambda k, s: up_sum.at[0, :, k, pl.ds(s * 64, 64), :],
                lambda d: far_one.at[0, 0, d], lambda d, s: near_one.at[0, 0, d, s],
            ),
        ],
        SIDE * 64 * HALF, bulk, sems, next(sums),
    )
    lines, second_sums = [], []
    for q in (2, 1, -1, 0):
        z, x = around(place.z + q), around(place.x + q)
        lines.append(RingSum(
            place,
            [
                (
                    "z", lambda k, s, x=x: down_sum.at[1, k, x, pl.ds(s * 64, 64), :],
                    lambda d, x=x: far_one.at[1, 1, d, x], lambda d, s, x=x: near_one.at[1, 1, d, s, x],
                ),
                (
                    "x", lambda k, s, z=z: up_sum.at[1, z, k, pl.ds(s * 64, 64), :],
                    lambda d, z=z: far_one.at[0, 1, d, z], lambda d, s, z=z: near_one.at[0, 1, d, s, z],
                ),
            ],
            64 * HALF, bulk, sems, next(sums),
        ))
    for h in range(2):
        second_sums.append(RingSum(
            place,
            [
                (
                    "x", lambda k, s, h=h: down_sum.at[h, place.z, k, pl.ds(s * 64, 64), :],
                    lambda d, h=h: far_two.at[1, h, d], lambda d, s, h=h: near_two.at[1, h, d, s],
                ),
                (
                    "z", lambda k, s, h=h: up_sum.at[h, k, place.x, pl.ds(s * 64, 64), :],
                    lambda d, h=h: far_two.at[0, h, d], lambda d, s, h=h: near_two.at[0, h, d, s],
                ),
            ],
            64 * HALF, bulk, sems, next(sums),
        ))

    order = [around(place.y + d) for d in (2, 1, -1, 0)]

    def swap(a, i):
        return remote(
            part.at[a, 1 - place.core, order[i]], other.at[a, order[i]], place.device(core=1),
            send_sem.at[3], pair_recv.at[4 + 3 * a + (0, 1, 2, 2)[i]],
        )

    def sent(i, count):
        ref = act.at[:, pl.ds(0, count // (3 * MODEL)), :]
        remote(ref, ref, place.device(core=1), send_sem.at[i], pair_recv.at[0]).wait_send()

    def strip(m):
        return pl.ds(pl.multiple_of(m * STRIP, STRIP), STRIP)

    def columns(h):
        return pl.ds(h * HALF, HALF)

    def turn(a, core, start, stop):
        @pl.loop(start, stop)
        def _(d):
            block = pl.ds(pl.multiple_of((around(place.y + d) * 2 + core) * WIDTH, WIDTH), WIDTH)
            turned[a, block, :] = act[a, :, block].T

    def up_of(h):
        return up[h].reshape(MODEL, HALF)

    def earlier_up(h):
        @pl.loop(0, 2)
        def _(m):
            value = jnp.maximum(dot(act[0, strip(m), :], up_of(h)), 0.0)
            first_up[strip(m), :] = value
            early_hidden[strip(m), columns(h)] = jnp.square(value).astype(bf16)

    def hidden_grad(h):
        @pl.loop(0, 2)
        def _(m):
            value = dot_turned(act[1, strip(m), :], down[columns(h), :])
            grad[strip(m), columns(h)] = (2.0 * first_up[strip(m), :] * value).astype(bf16)

    def weight_grad(a, source, target, h):
        @pl.loop(0, 4)
        def _(n):
            block = pl.ds(pl.multiple_of(n * 512, 512), 512)
            value = dot(turned[a, block, :], source[:, columns(h)])
            target[h, n] = value.astype(bf16).reshape(SIDE, 128, HALF)

    def later_up(h):
        @pl.loop(0, 2)
        def _(m):
            value = dot(act[2, strip(m), :], up_of(h))
            pre[strip(m), columns(h)] = value.astype(bf16)
            hidden[strip(m), columns(h)] = jnp.square(jnp.maximum(value, 0.0)).astype(bf16)

    def keep(a, n, m, value):
        value = value.astype(bf16)
        part[a, 0, n, strip(m), :] = value[:, :WIDTH]
        part[a, 1, n, strip(m), :] = value[:, WIDTH:]

    def later_out(i):
        n = order[i]
        block = pl.ds(pl.multiple_of(n * 512, 512), 512)

        @pl.loop(0, 2)
        def _(m):
            keep(0, n, m, dot(hidden[strip(m), :], down[:, block]))

        swap(0, i).start()

    def input_grad(i):
        n = order[i]

        @pl.loop(0, 2)
        def _(m):
            weight = jnp.concatenate([up[h, n].reshape(512, HALF) for h in range(2)], axis=1)
            keep(1, n, m, dot_turned(grad[strip(m), :], weight))

        swap(1, i).start()

    def join(a, i):
        if i == 2:
            ref = bulk(2 * ROWS * WIDTH)
            remote(ref, ref, place.device(core=1), send_sem.at[3], pair_recv.at[6 + 3 * a]).wait_recv()
        elif i < 2:
            swap(a, i).wait_recv()
        n = order[i]
        part[a, place.core, n] = (
            part[a, place.core, n].astype(f32) + other[a, n].astype(f32)
        ).astype(bf16)
        row_sums[a].start(((0, 1), (2,), (3,), ())[i])

    def add_running(h):
        second_sums[h].arrive()
        for p, run in enumerate((down_run, up_run)):
            for s in range(2):
                at = run.at[pl.ds(s * 64, 64), columns(h)]
                at[...] = at[...] + second_sums[h].total(p, s) * factor

    pl.semaphore_wait(barrier, 7)
    loaded(0, 128 * HALF + HIDDEN * 128)

    first[0].own()
    second[0].own()
    loaded(1, ROWS * WIDTH)
    rows[0].own()
    pairs[0].start(0)
    loaded(2, 128 * HALF + 2 * ROWS * WIDTH + 4 * 128 * HIDDEN)
    first[0].forward()
    first[1].own()
    first[0].near()
    second[1].own()
    second[2].own()
    second[0].forward()
    rows[0].forward()
    rows[1].own()
    pairs[1].start(0)
    first[0].far()
    second[3].own()
    first[1].forward()
    second[1].forward()
    rows[0].near()
    pairs[0].start(1, 2)
    rows[0].far()
    pairs[0].start(3)
    second[2].forward()
    second[3].forward()
    rows[1].forward()
    rows[2].own()
    pairs[2].start(0)
    first[1].rest()
    last.own()
    pairs[0].wait(0, 4)
    turn(0, place.core, -1, 3)
    turn(0, 1 - place.core, -1, 3)
    rows[1].near()
    pairs[1].start(1, 2)
    for ring in second:
        ring.rest()
    earlier_up(0)
    rows[1].far()
    pairs[1].start(3)
    turn(1, place.core, -1, 3)
    pairs[1].wait(0, 3)
    turn(1, 1 - place.core, -1, 2)
    pairs[1].wait(1, 1)
    turn(1, 1 - place.core, 2, 3)
    rows[2].forward()
    last.forward()
    weight_grad(1, early_hidden, down_sum, 0)
    first_sum.begin(0)
    hidden_grad(0)
    rows[2].near()
    pairs[2].start(1, 2)
    weight_grad(0, grad, up_sum, 0)
    first_sum.begin(1)
    rows[2].far()
    pairs[2].start(3)
    pairs[2].wait(0, 4)
    later_up(0)
    last.rest()
    earlier_up(1)
    hidden_grad(1)
    input_grad(0)
    input_grad(1)
    first_sum.middle()
    weight_grad(1, early_hidden, down_sum, 1)
    for which in ((0, 1), (2, 3)):
        for line in lines[:3]:
            line.start(which, (0,))
    join(1, 0)
    weight_grad(0, grad, up_sum, 1)
    for which in ((0, 1), (2, 3)):
        for line in lines[:3]:
            line.start(which, (1,))
    join(1, 1)
    input_grad(2)
    input_grad(3)
    later_up(1)
    join(1, 2)
    join(1, 3)
    first_sum.finish()
    second_sums[0].start((0, 1))
    row_sums[1].middle()
    later_out(0)
    later_out(1)
    later_out(2)
    join(0, 0)
    for line in lines[:3]:
        line.middle()
    lines[3].start((0, 1))
    second_sums[0].start((2, 3))
    later_out(3)
    join(0, 1)
    join(0, 2)
    join(0, 3)
    lines[0].finish()
    second_sums[1].start((0, 1))
    lines[3].start((2, 3))
    second_sums[0].middle()
    row_sums[1].finish(back_out)
    lines[1].finish()
    lines[2].finish()
    second_sums[1].start((2, 3))
    row_sums[0].middle()
    lines[3].middle()
    second_sums[1].middle()
    add_running(0)
    row_sums[0].finish(later_out_ref)
    lines[3].finish()
    add_running(1)
    sent(0, 120 * 64 * HALF)
    sent(1, 120 * 64 * HALF)
    sent(2, 18 * STRIP * WIDTH + 12 * ROWS * WIDTH)
    sent(3, 12 * STRIP * WIDTH + 8 * ROWS * WIDTH)


def store_kernel(*refs):
    sources, results, sem = refs[:5], refs[5:10], refs[10]
    copies = [
        pltpu.make_async_copy(src, dst, sem.at[i]) for i, (src, dst) in enumerate(zip(sources, results))
    ]
    for copy in copies:
        copy.start()
    for copy in copies:
        copy.wait()


def on_device(*arrays):
    factor = float(ROWS * 16) ** (-0.5)
    anywhere = pl.BlockSpec(memory_space=pl.ANY)
    inside = pl.BlockSpec(memory_space=pltpu.VMEM)
    kept = [
        ((ROWS, WIDTH), bf16),
        ((ROWS, HIDDEN), bf16),
        ((ROWS, WIDTH), bf16),
        ((128, HIDDEN), f32),
        ((128, HIDDEN), f32),
    ]
    results = pl.pallas_call(
        lambda *refs: layer_kernel(factor, *refs),
        out_shape=tuple(pltpu.VMEM(shape, kind) for shape, kind in kept),
        in_specs=[anywhere] * 7,
        out_specs=(inside,) * 5,
        scratch_shapes=[
            pltpu.VMEM((3, ROWS, MODEL), bf16),
            pltpu.VMEM((2, MODEL, ROWS), bf16),
            pltpu.VMEM((2, SIDE, SIDE, 128, HALF), bf16),
            pltpu.VMEM((HIDDEN, MODEL), bf16),
            pltpu.VMEM((ROWS, HALF), f32),
            pltpu.VMEM((ROWS, HIDDEN), bf16),
            pltpu.VMEM((ROWS, HIDDEN), bf16),
            pltpu.VMEM((ROWS, HIDDEN), bf16),
            pltpu.VMEM((2, 2, SIDE, ROWS, WIDTH), bf16),
            pltpu.VMEM((2, SIDE, ROWS, WIDTH), bf16),
            pltpu.VMEM((2, SIDE, SIDE, 128, HALF), bf16),
            pltpu.VMEM((2, SIDE, SIDE, 128, HALF), bf16),
            pltpu.VMEM((2, 2, STRIP, WIDTH), bf16),
            pltpu.VMEM((2, 2, 2, STRIP, WIDTH), bf16),
            pltpu.VMEM((2, 2, 2, SIDE, 64, HALF), bf16),
            pltpu.VMEM((2, 2, 2, 2, SIDE, 64, HALF), bf16),
            pltpu.VMEM((2, 2, 2, 64, HALF), bf16),
            pltpu.VMEM((2, 2, 2, 2, 64, HALF), bf16),
            pltpu.SemaphoreType.DMA((3,)),
            pltpu.SemaphoreType.DMA((4,)),
            pltpu.SemaphoreType.DMA((24,)),
            pltpu.SemaphoreType.DMA((10,)),
            pltpu.SemaphoreType.DMA((18,)),
        ],
        compiler_params=pltpu.CompilerParams(
            collective_id=0, has_side_effects=True, vmem_limit_bytes=LIMIT
        ),
    )(*arrays)
    return pl.pallas_call(
        store_kernel,
        out_shape=tuple(jax.ShapeDtypeStruct(shape, kind) for shape, kind in kept),
        in_specs=[inside] * 5,
        out_specs=(anywhere,) * 5,
        scratch_shapes=[pltpu.SemaphoreType.DMA((5,))],
        compiler_params=pltpu.CompilerParams(vmem_limit_bytes=2**20),
    )(*[pltpu.with_memory_space_constraint(r, pltpu.VMEM) for r in results])


def solution(mesh):
    in_specs = (
        P("fs", "tp"),
        P("fs", "tp"),
        P("fs", "tp"),
        P("fs", "tp"),
        P("tp", "fs"),
        P("fs", "tp"),
        P("fs", "tp"),
    )
    out_specs = (P("fs", "tp"),) * 5
    return jax.shard_map(
        on_device, mesh=mesh, in_specs=in_specs, out_specs=out_specs, check_vma=False
    )
```

time: 97.5 us -> 95.3 us (0.977)
  Pallas kernels: 96.8 us -> 94.4 us
    pallas_call x1, Pallas kernels: 95 us -> 92.6 us  [on_device(): pl.pallas_call(lambda *refs: layer_kernel(factor, *refs), out_shape=tuple...]
where the time goes in v6:
time: 95.3 us; the launch traced here: 95.1 us
  Pallas kernels  94.4 us (99%)
    pallas_call x1, Pallas kernels, on_device(): pl.pallas_call(lambda *refs: layer_kernel(factor, *refs), out_shape=tuple...  92.6 us

profile of v6, /device:TPU:0, one launch (start us, length us, event | category | flops | bytes accessed | tf_op | source)
XLA Modules:
  0.0 95.1 jit_solution(8418719321650278236)
XLA Ops:
  0.6 92.6 %shard_map.110 = (bf16[768,256]{1,0:T(8,128)(2,1)S(1)}, bf16[768,1024]{1,0:T(8,128)(2,1)S(1)}, bf16[768,256]{1,0:T(8,128)(2,1)S(1)}, f32[128,1024]{1,0:T(8,128)S(1)}, f32[128,1024]{1,0:T(8,128)S(1)}) custom-call(bf16[768,256]{1,0:T(8,128)(2,1)} %refs_0_.1, bf16[768,256]{1,0:T(8,128)(2,1)} %refs_1_.1, bf16[768,256]{1,0:T(8,128)(2,1)} %refs_2_.1, ...), custom_call_target="tpu_custom_call" | custom-call | tf_op jit(solution)/shard_map/pallas_call | solution.py:569
  93.3 1.8 %shard_map.111 = (bf16[768,256]{1,0:T(8,128)(2,1)}, bf16[768,1024]{1,0:T(8,128)(2,1)}, bf16[768,256]{1,0:T(8,128)(2,1)}, f32[128,1024]{1,0:T(8,128)}, f32[128,1024]{1,0:T(8,128)}) custom-call(bf16[768,256]{1,0:T(8,128)(2,1)S(1)} %get-tuple-element.10.refs_0_, bf16[768,1024]{1,0:T(8,128)(2,1)S(1)} %get-tuple-element.11.refs_1_, ...), custom_call_target="tpu_custom_call" | custom-call | tf_op jit(solution)/shard_map/pallas_call | solution.py:603

commit v7 on v6

--- a/solution.py
+++ b/solution.py
@@ -6,7 +6,6 @@
 from jax.sharding import PartitionSpec as P
 
 contract_last = (((1,), (1,)), ((), ()))
-contract_first = (((0,), (0,)), ((), ()))
 bf16, f32 = jnp.bfloat16, jnp.float32
 MESH = pl.DeviceIdType.MESH
 SIDE = 4
@@ -44,11 +43,11 @@
 
 
 class Ring:
-    def __init__(self, place, parts, half, bulk, sems, bases, joint=False):
+    def __init__(self, place, parts, half, bulk, sems, bases, joint=False, shared=None):
         self.place, self.count, self.bulk, self.sems = place, half * len(parts), bulk, sems
-        self.last = 1 if joint else 2
-        self.base = bases[0]
-        del bases[: self.last + 1]
+        self.base = bases.pop(0)
+        self.side = bases.pop(0) if shared is None else shared
+        self.last = self.side if joint else bases.pop(0)
         self.sent = []
         for axis, piece in parts:
             at = getattr(place, axis)
@@ -68,29 +67,29 @@
         for part in self.sent:
             for j in which:
                 ref, device = part[j]
-                k = (0, 1, 0, 1, self.last, self.last)[j]
-                remote(ref, ref, device, send, receive.at[self.base + k]).start()
+                k = (self.base, self.side, self.base, self.side, self.last, self.last)[j]
+                remote(ref, ref, device, send, receive.at[k]).start()
 
     def wait(self, k, halves):
         send, receive = self.sems
         ref = self.bulk(halves * self.count)
-        remote(ref, ref, self.place.device(core=1), send, receive.at[self.base + k]).wait_recv()
+        remote(ref, ref, self.place.device(core=1), send, receive.at[k]).wait_recv()
 
     def own(self):
         self.start(0, 2, 1, 3)
 
     def forward(self):
-        self.wait(0, 2)
+        self.wait(self.base, 2)
         self.start(4, 5)
 
     def near(self):
-        self.wait(1, 2)
+        self.wait(self.side, 2)
 
     def far(self):
-        self.wait(2, 2)
-
-    def rest(self):
-        self.wait(1, 4)
+        self.wait(self.last, 2)
+
+    def rest(self, rings=1):
+        self.wait(self.side, 4 * rings)
 
 
 class Partner:
@@ -223,7 +222,7 @@
         ref = bulk(count)
         pltpu.make_async_copy(ref, ref, load_sem.at[k]).wait()
 
-    bases = list(range(24))
+    bases = list(range(21))
     sems = (send_sem.at[0], ring_recv)
     rows = [
         Ring(
@@ -257,7 +256,7 @@
                 ("x", lambda k, s, z=z: up.at[0, z, k, pl.ds(s * 64, 64), :]),
                 ("z", lambda k, s, x=x: down_at(0, s, k * SIDE + x, 128)),
             ],
-            64 * HALF, bulk, sems, bases, True,
+            64 * HALF, bulk, sems, bases, True, second[0].side if second else None,
         ))
     last = Ring(
         place,
@@ -434,8 +433,8 @@
     loaded(1, ROWS * WIDTH)
     rows[0].own()
     pairs[0].start(0)
+    first[0].forward()
     loaded(2, 128 * HALF + 2 * ROWS * WIDTH + 4 * 128 * HIDDEN)
-    first[0].forward()
     first[1].own()
     first[0].near()
     second[1].own()
@@ -464,8 +463,7 @@
     turn(0, 1 - place.core, -1, 3)
     rows[1].near()
     pairs[1].start(1, 2)
-    for ring in second:
-        ring.rest()
+    second[0].rest(4)
     earlier_up(0)
     rows[1].far()
     pairs[1].start(3)
@@ -549,8 +547,8 @@
     copies = [
         pltpu.make_async_copy(src, dst, sem.at[i]) for i, (src, dst) in enumerate(zip(sources, results))
     ]
-    for copy in copies:
-        copy.start()
+    for i in (1, 3, 4, 0, 2):
+        copies[i].start()
     for copy in copies:
         copy.wait()
 
@@ -592,7 +590,7 @@
             pltpu.VMEM((2, 2, 2, 2, 64, HALF), bf16),
             pltpu.SemaphoreType.DMA((3,)),
             pltpu.SemaphoreType.DMA((4,)),
-            pltpu.SemaphoreType.DMA((24,)),
+            pltpu.SemaphoreType.DMA((21,)),
             pltpu.SemaphoreType.DMA((10,)),
             pltpu.SemaphoreType.DMA((18,)),
         ],

time: 95.3 us -> 95.3 us (level)
  no operation moved by 1% of the time
where the time goes in v7:
time: 95.3 us; the launch traced here: 95 us
  Pallas kernels  94.4 us (99%)
    pallas_call x1, Pallas kernels, on_device(): pl.pallas_call(lambda *refs: layer_kernel(factor, *refs), out_shape=tuple...  92.6 us

profile of v7, /device:TPU:0, one launch (start us, length us, event | category | flops | bytes accessed | tf_op | source)
XLA Modules:
  0.0 95.0 jit_solution(5041311846302088401)
XLA Ops:
  0.6 92.6 %shard_map.110 = (bf16[768,256]{1,0:T(8,128)(2,1)S(1)}, bf16[768,1024]{1,0:T(8,128)(2,1)S(1)}, bf16[768,256]{1,0:T(8,128)(2,1)S(1)}, f32[128,1024]{1,0:T(8,128)S(1)}, f32[128,1024]{1,0:T(8,128)S(1)}) custom-call(bf16[768,256]{1,0:T(8,128)(2,1)} %refs_0_.1, bf16[768,256]{1,0:T(8,128)(2,1)} %refs_1_.1, bf16[768,256]{1,0:T(8,128)(2,1)} %refs_2_.1, ...), custom_call_target="tpu_custom_call" | custom-call | tf_op jit(solution)/shard_map/pallas_call | solution.py:567
  93.3 1.8 %shard_map.111 = (bf16[768,256]{1,0:T(8,128)(2,1)}, bf16[768,1024]{1,0:T(8,128)(2,1)}, bf16[768,256]{1,0:T(8,128)(2,1)}, f32[128,1024]{1,0:T(8,128)}, f32[128,1024]{1,0:T(8,128)}) custom-call(bf16[768,256]{1,0:T(8,128)(2,1)S(1)} %get-tuple-element.10.refs_0_, bf16[768,1024]{1,0:T(8,128)(2,1)S(1)} %get-tuple-element.11.refs_1_, ...), custom_call_target="tpu_custom_call" | custom-call | tf_op jit(solution)/shard_map/pallas_call | solution.py:601

commit v8 on v7

--- a/solution.py
+++ b/solution.py
@@ -523,14 +523,14 @@
     join(0, 3)
     lines[0].finish()
     second_sums[1].start((0, 1))
-    lines[3].start((2, 3))
     second_sums[0].middle()
     row_sums[1].finish(back_out)
     lines[1].finish()
     lines[2].finish()
+    lines[3].start((2, 3))
     second_sums[1].start((2, 3))
+    lines[3].middle()
     row_sums[0].middle()
-    lines[3].middle()
     second_sums[1].middle()
     add_running(0)
     row_sums[0].finish(later_out_ref)

time: 95.3 us -> 95.3 us (level)
  no operation moved by 1% of the time
where the time goes in v8:
time: 95.3 us; the launch traced here: 95 us
  Pallas kernels  94.4 us (99%)
    pallas_call x1, Pallas kernels, on_device(): pl.pallas_call(lambda *refs: layer_kernel(factor, *refs), out_shape=tuple...  92.6 us

profile of v8, /device:TPU:0, one launch (start us, length us, event | category | flops | bytes accessed | tf_op | source)
XLA Modules:
  0.0 95.0 jit_solution(18148143637729375635)
XLA Ops:
  0.6 92.6 %shard_map.110 = (bf16[768,256]{1,0:T(8,128)(2,1)S(1)}, bf16[768,1024]{1,0:T(8,128)(2,1)S(1)}, bf16[768,256]{1,0:T(8,128)(2,1)S(1)}, f32[128,1024]{1,0:T(8,128)S(1)}, f32[128,1024]{1,0:T(8,128)S(1)}) custom-call(bf16[768,256]{1,0:T(8,128)(2,1)} %refs_0_.1, bf16[768,256]{1,0:T(8,128)(2,1)} %refs_1_.1, bf16[768,256]{1,0:T(8,128)(2,1)} %refs_2_.1, ...), custom_call_target="tpu_custom_call" | custom-call | tf_op jit(solution)/shard_map/pallas_call | solution.py:567
  93.3 1.8 %shard_map.111 = (bf16[768,256]{1,0:T(8,128)(2,1)}, bf16[768,1024]{1,0:T(8,128)(2,1)}, bf16[768,256]{1,0:T(8,128)(2,1)}, f32[128,1024]{1,0:T(8,128)}, f32[128,1024]{1,0:T(8,128)}) custom-call(bf16[768,256]{1,0:T(8,128)(2,1)S(1)} %get-tuple-element.10.refs_0_, bf16[768,1024]{1,0:T(8,128)(2,1)S(1)} %get-tuple-element.11.refs_1_, ...), custom_call_target="tpu_custom_call" | custom-call | tf_op jit(solution)/shard_map/pallas_call | solution.py:601
